TPU v7x, 256 devices: a whole 4x4x8 slice. The times are simulated.
256 devices in a mesh: sp: 32 (over z, x), tp: 8 (over y, core).
Axes of the slice: x: 4, y: 4, z: 8, core: 2. Of those that a mesh axis runs over, the one named last changes fastest.
Arguments:
- tokens: bfloat16 [32768, 2048], P('sp'), may hold values from -6 to 6
- pre_gain: float32 [2048], replicated, may hold values from 0.1 to 1.9
- w_query: bfloat16 [2048, 2048], P(None, 'tp'), may hold values from -0.125 to 0.125
- w_key: bfloat16 [2048, 2048], P(None, 'tp'), may hold values from -0.125 to 0.125
- w_value: bfloat16 [2048, 2048], P(None, 'tp'), may hold values from -0.125 to 0.125
- memory_output_gate_weight: bfloat16 [2048, 2048], P(None, 'tp'), may hold values from -0.125 to 0.125
- w_input_gate: bfloat16 [2048, 8], replicated, may hold values from -0.125 to 0.125
- w_forget_gate: bfloat16 [2048, 8], replicated, may hold values from -0.125 to 0.125
- input_bias: float32 [8], replicated, may hold values from -3 to 220
- forget_bias: float32 [8], replicated, may hold values from 3.9 to 12.4
- forget_extra: float32 [32768, 8], P('sp', 'tp'), may hold values from -1.5 to 0
- initial_memory: float32 [8, 256, 256], P('tp', 'sp'), may hold values from -4096 to 4096
- initial_normal: float32 [8, 256], P('tp', 'sp'), may hold values from -4096 to 4096
- memory_gain: float32 [2048], replicated, may hold values from 0.1 to 1.9
- w_pool_input: bfloat16 [2048, 1024], P(None, 'tp'), may hold values from -0.125 to 0.125
- w_pool_gate: bfloat16 [2048, 1024], P(None, 'tp'), may hold values from -0.125 to 0.125
- pool_mix: bfloat16 [8, 128, 128], replicated, may hold values from -0.5 to 0.5
- pool_gain: float32 [1024], replicated, may hold values from 0.1 to 1.9
- w_out_memory: bfloat16 [2048, 2048], P('tp'), may hold values from -0.109375 to 0.109375
- w_out_pool: bfloat16 [1024, 2048], P('tp'), may hold values from -0.109375 to 0.109375
- post_gain: float32 [2048], replicated, may hold values from 0.1 to 1.9
Outputs:
- layer_out: bfloat16 [32768, 2048], P(('sp', 'tp'))
All inputs are finite; a program needn't handle non-finite values.
Results may differ from a plain program's by a relative error of at most 0.018.
The roundings to bfloat16 on the way count: a program that leaves them out, or rounds other values in their place, can miss the bound.
Values may be sent and summed in bfloat16 or wider, within the bound.
A program may use at most 128 MiB of HBM per device.

v0:
```python
import jax
import jax.numpy as jnp
from jax import lax
from jax.sharding import PartitionSpec as P

HEAD_DIM = 256
MEM_WIDTH = 2048
GROUP_DIM = 128
WIDEST = 256
BLOCK = 512


EPS = 1e-06
FLOOR = -1e30


def sent_together(arrays, axis, dim, along):
    columns = [a.reshape(*a.shape[:along], -1) for a in arrays]
    both = jnp.concatenate(columns, axis=along)
    result, at, finished = (lax.all_gather(both, axis, axis=dim, tiled=True), 0, [])
    for a, column in zip(arrays, columns):
        slab = result[..., at : at + column.shape[along]]
        finished.append(slab.reshape(*slab.shape[:along], *a.shape[along:]))
        at += column.shape[along]
    return tuple(finished)


def sent_to_all(value, axis):
    copies = jnp.broadcast_to(value, (lax.axis_size(axis), *value.shape))
    return lax.all_to_all(copies, axis, split_axis=0, concat_axis=0, tiled=True)


def in_order(blocks, dim):
    lengths = list(blocks.shape[1:])
    lengths[dim] *= blocks.shape[0]
    return jnp.moveaxis(blocks, 0, dim).reshape(lengths)


def gathered_copies(value, axis, dim):
    blocks = sent_to_all(value, axis)
    return in_order(blocks, dim)


def passed_along(value, axis, steps):
    count = lax.axis_size(axis)
    first, last = (max(0, -steps), min(count, count - steps))
    return lax.ppermute(value, axis, [(source, source + steps) for source in range(first, last)])


def normalize(values, gain):
    return values * lax.rsqrt(jnp.mean(values * values, axis=-1, keepdims=True) + EPS) * gain


def block_parts(memory_carry, block_inputs):
    matrix_memory_state, memory_normal, stabilizer = memory_carry
    queries, keys_in, incoming_values, log_input, log_keep = block_inputs
    length = queries.shape[1]
    head_scale = queries.shape[2] ** (-0.5)
    causal = jnp.arange(length)[:, None] >= jnp.arange(length)[None, :]
    running_keep = jnp.cumsum(log_keep, axis=-1)
    decayed = jnp.where(
        causal[None],
        running_keep[:, :, None] - running_keep[:, None, :] + log_input[:, None, :],
        -jnp.inf,
    )
    carried = running_keep + stabilizer[:, None]
    row_max = jnp.maximum(jnp.max(decayed, axis=-1), carried)
    wide_queries = queries.astype(jnp.float32)
    scores = jnp.einsum("hld,hsd->hls", queries, keys_in, preferred_element_type=jnp.float32)
    weights = jnp.exp(decayed - row_max[:, :, None]) * scores * head_scale
    carry_weight = jnp.exp(carried - row_max) * head_scale
    numerator = jnp.einsum(
        "hls,hsd->hld",
        weights.astype(jnp.bfloat16),
        incoming_values,
        preferred_element_type=jnp.float32,
    )
    numerator = numerator + carry_weight[:, :, None] * jnp.einsum(
        "hld,hde->hle", wide_queries, matrix_memory_state, precision=lax.Precision.HIGHEST
    )
    denominator = jnp.sum(weights, axis=-1) + carry_weight * jnp.einsum(
        "hld,hd->hl", wide_queries, memory_normal, precision=lax.Precision.HIGHEST
    )
    block_keep = running_keep[:, -1]
    write_log = block_keep[:, None] - running_keep + log_input
    new_stabilizer = jnp.maximum(block_keep + stabilizer, jnp.max(write_log, axis=-1))
    decay_factor = jnp.exp(block_keep + stabilizer - new_stabilizer)
    write_weight = jnp.exp(write_log - new_stabilizer[:, None])
    key_projected = write_weight[:, :, None] * keys_in.astype(jnp.float32)
    matrix_memory_state = decay_factor[:, None, None] * matrix_memory_state + jnp.einsum(
        "gbq,gbd->gqd",
        key_projected.astype(jnp.bfloat16),
        incoming_values,
        preferred_element_type=jnp.float32,
    )
    memory_normal = decay_factor[:, None] * memory_normal + jnp.sum(key_projected, axis=1)
    return ((matrix_memory_state, memory_normal, new_stabilizer), (numerator, denominator, row_max))


def body(
    tokens,
    pre_gain,
    w_query,
    w_key,
    w_value,
    memory_output_gate_weight,
    w_input_gate,
    w_forget_gate,
    input_bias,
    forget_bias,
    forget_extra,
    initial_memory,
    initial_normal,
    memory_gain,
    w_pool_input,
    w_pool_gate,
    pool_mix,
    pool_gain,
    w_out_memory,
    w_out_pool,
    post_gain,
):
    token_count = tokens.shape[0]
    local_heads = w_query.shape[1] // HEAD_DIM
    local_groups = w_pool_input.shape[1] // GROUP_DIM
    head_index = lax.axis_index("tp")
    first_head = head_index * local_heads
    first_group = head_index * local_groups
    normed = normalize(tokens.astype(jnp.float32), pre_gain).astype(jnp.bfloat16)

    def by_heads(weight):
        shaped = weight.reshape(weight.shape[0], local_heads, HEAD_DIM)
        return jnp.einsum("td,dhe->hte", normed, shaped, preferred_element_type=jnp.float32)

    queries = by_heads(w_query).astype(jnp.bfloat16)
    keys_all = by_heads(w_key).astype(jnp.bfloat16)
    values_all = by_heads(w_value).astype(jnp.bfloat16)
    memory_gate = by_heads(memory_output_gate_weight)
    input_cols = lax.dynamic_slice_in_dim(w_input_gate, first_head, local_heads, 1)
    forget_cols = lax.dynamic_slice_in_dim(w_forget_gate, first_head, local_heads, 1)
    input_shift = lax.dynamic_slice_in_dim(input_bias, first_head, local_heads, 0)
    forget_shift = lax.dynamic_slice_in_dim(forget_bias, first_head, local_heads, 0)
    log_input = (jnp.dot(normed, input_cols, preferred_element_type=jnp.float32) + input_shift).T
    log_keep = (
        jax.nn.log_sigmoid(
            jnp.dot(normed, forget_cols, preferred_element_type=jnp.float32) + forget_shift
        )
        + forget_extra
    ).T
    block_total = token_count // BLOCK

    def split(array):
        return jnp.moveaxis(
            array.reshape((local_heads, block_total, BLOCK) + array.shape[2:]), 1, 0
        )

    def join(array):
        return jnp.moveaxis(array, 0, 1).reshape((local_heads, token_count) + array.shape[3:])

    empty_state = jnp.zeros((local_heads, HEAD_DIM, HEAD_DIM), jnp.float32)
    empty_normal = jnp.zeros((local_heads, HEAD_DIM), jnp.float32)
    empty_stab = jnp.full((local_heads,), FLOOR, jnp.float32)
    summary, (numerator, denominator, row_max) = lax.scan(
        block_parts,
        (empty_state, empty_normal, empty_stab),
        (split(queries), split(keys_all), split(values_all), split(log_input), split(log_keep)),
    )
    summary_state, summary_normal, summary_stab = summary
    numerator, denominator, row_max = (join(numerator), join(denominator), join(row_max))
    keep_total = jnp.sum(log_keep, axis=1)
    keep_running = jnp.cumsum(log_keep, axis=1)
    start_memory, start_normal = sent_together((initial_memory, initial_normal), "sp", 1, 2)
    totals = gathered_copies(keep_total[None, :], "sp", 0)
    position = lax.axis_index("sp")
    block_ends = jnp.cumsum(totals, axis=0)
    earlier_rows = jnp.arange(totals.shape[0])[:, None] < position
    before_mine = jnp.sum(jnp.where(earlier_rows, totals, 0.0), axis=0)
    held_state = start_memory
    held_normal = start_normal
    piece_state, piece_normal, piece_stab = sent_together(
        (summary_state[None], summary_normal[None], summary_stab[None]), "sp", 0, 2
    )
    piece_count = piece_stab.shape[0]
    shard_index = jnp.arange(piece_count)
    earlier_piece = (shard_index < position)[:, None]
    log_weight = jnp.where(earlier_piece, piece_stab + before_mine[None, :] - block_ends, FLOOR)
    new_stab = jnp.maximum(before_mine, jnp.max(log_weight, axis=0))
    piece_weight = jnp.where(earlier_piece, jnp.exp(log_weight - new_stab[None, :]), 0.0)
    held_fade = jnp.exp(before_mine - new_stab)
    held_state = held_fade[:, None, None] * held_state + jnp.einsum(
        "kh,khij->hij", piece_weight, piece_state, precision=lax.Precision.HIGHEST
    )
    held_normal = held_fade[:, None] * held_normal + jnp.einsum(
        "kh,khi->hi", piece_weight, piece_normal, precision=lax.Precision.HIGHEST
    )
    head_scale = HEAD_DIM ** (-0.5)
    carried = keep_running + new_stab[:, None]
    joint_max = jnp.maximum(row_max, carried)
    local_weight = jnp.exp(row_max - joint_max)
    carry_weight = jnp.exp(carried - joint_max) * head_scale
    wide_queries = queries.astype(jnp.float32)
    numerator = numerator * local_weight[:, :, None] + carry_weight[:, :, None] * jnp.einsum(
        "hld,hde->hle", wide_queries, held_state, precision=lax.Precision.HIGHEST
    )
    denominator = denominator * local_weight + carry_weight * jnp.einsum(
        "hld,hd->hl", wide_queries, held_normal, precision=lax.Precision.HIGHEST
    )
    memory_rows = numerator / jnp.maximum(jnp.abs(denominator), jnp.exp(-joint_max))[:, :, None]
    local_squares = jnp.sum(memory_rows * memory_rows, axis=(0, 2))
    all_squares = lax.psum(local_squares, "tp")
    row_scale = lax.rsqrt(all_squares / MEM_WIDTH + EPS)
    gain_local = lax.dynamic_slice_in_dim(
        memory_gain, first_head * HEAD_DIM, local_heads * HEAD_DIM, 0
    ).reshape(local_heads, 1, HEAD_DIM)
    memory_out = (
        memory_rows * row_scale[None, :, None] * gain_local * jax.nn.silu(memory_gate)
    ).astype(jnp.bfloat16)
    pool_input = jnp.dot(normed, w_pool_input, preferred_element_type=jnp.float32).astype(
        jnp.bfloat16
    )
    rim_rows = passed_along(pool_input[token_count - WIDEST :], "sp", 1)
    extended = jnp.concatenate([rim_rows, pool_input], axis=0)
    group_ids = first_group + jnp.arange(local_groups)
    windows = jnp.left_shift(2, group_ids)
    target_rows = jnp.arange(token_count)[:, None]
    source_rows = jnp.arange(token_count + WIDEST)[None, :] - WIDEST
    inside = (source_rows <= target_rows)[None] & (
        source_rows[None] > target_rows[None] - windows[:, None, None]
    )
    band = inside.astype(jnp.bfloat16)
    window_sums = jnp.einsum(
        "gts,sgc->tgc",
        band,
        extended.reshape(token_count + WIDEST, local_groups, GROUP_DIM),
        preferred_element_type=jnp.float32,
    )
    global_rows = lax.axis_index("sp") * token_count + jnp.arange(token_count)
    counts = jnp.minimum(global_rows[:, None] + 1, windows[None, :]).astype(jnp.float32)
    grouped = pool_input.astype(jnp.float32).reshape(token_count, local_groups, GROUP_DIM)
    pooled = (window_sums / counts[:, :, None] - grouped).astype(jnp.bfloat16)
    mix_local = lax.dynamic_slice_in_dim(pool_mix, first_group, local_groups, 0)
    mixed = jnp.einsum("tgc,gce->tge", pooled, mix_local, preferred_element_type=jnp.float32)
    pool_gate = jnp.dot(normed, w_pool_gate, preferred_element_type=jnp.float32)
    pool_scale = lax.dynamic_slice_in_dim(
        pool_gain, first_group * GROUP_DIM, local_groups * GROUP_DIM, 0
    )
    pool_out = (
        mixed.reshape(token_count, local_groups * GROUP_DIM) * pool_scale * jax.nn.silu(pool_gate)
    ).astype(jnp.bfloat16)
    out_memory = w_out_memory.reshape(local_heads, HEAD_DIM, w_out_memory.shape[1])
    memory_term = jnp.einsum(
        "hte,hed->td", memory_out, out_memory, preferred_element_type=jnp.float32
    )
    summed = lax.psum_scatter(
        (memory_term + jnp.dot(pool_out, w_out_pool, preferred_element_type=jnp.float32)).astype(
            jnp.bfloat16
        ),
        "tp",
        scatter_dimension=0,
        tiled=True,
    ).astype(jnp.float32)
    return normalize(summed, post_gain).astype(jnp.bfloat16)


def solution(mesh):
    in_specs = (
        P("sp", None),
        P(),
        P(None, "tp"),
        P(None, "tp"),
        P(None, "tp"),
        P(None, "tp"),
        P(),
        P(),
        P(),
        P(),
        P("sp", "tp"),
        P("tp", "sp", None),
        P("tp", "sp"),
        P(),
        P(None, "tp"),
        P(None, "tp"),
        P(),
        P(),
        P("tp", None),
        P("tp", None),
        P(),
    )
    out_specs = P(("sp", "tp"), None)
    return jax.shard_map(body, mesh=mesh, in_specs=in_specs, out_specs=out_specs, check_vma=False)
```

profile of v0, /device:TPU:1, one launch (start us, length us, event | category | flops | bytes accessed | tf_op | source)
XLA Modules:
  0.0 250.7 jit_solution(17415238615556287580)
XLA Ops:
  6.6 3.2 %fusion.41 = f32[1024]{0:T(1024)S(1)} fusion(bf16[1024,2048]{1,0:T(8,128)(2,1)} %param.23), kind=kLoop, calls=%fused_computation.64 | loop fusion | flops 6290432 | bytes 4198400 | tf_op jit(solution)/shard_map/reduce_sum | solution.py:51
  9.8 3.2 %fusion.43 = bf16[1024,2048]{1,0:T(8,128)(2,1)S(1)} fusion(bf16[1024,2048]{1,0:T(8,128)(2,1)} %param.23, f32[2048]{0:T(1024)S(1)} %copy-done.7, f32[1024]{0:T(1024)S(1)} %add_rsqrt_fusion.1), kind=kLoop, calls=%fused_computation.66 | loop fusion | flops 8388608 | bytes 8400896 | tf_op jit(solution)/shard_map/convert_element_type | solution.py:129
  13.0 0.7 dynamic_slice.39
  13.7 2.1 fusion.109
  15.8 2.0 fusion.107
  17.8 0.7 dynamic_slice.41
  18.4 1.3 convolution_convert_fusion
  19.7 1.3 convolution_convert_fusion.2
  21.0 1.3 convolution_convert_fusion.1
  22.3 0.6 fusion.111
  22.9 0.7 fusion.125
  23.6 0.7 broadcast_add_fusion
  24.3 15.9 %while.21 = (s32[]{:T(128)}, f32[1,256,256]{2,1,0:T(8,128)S(1)}, f32[1,256]{1,0:T(1,128)S(1)}, f32[1]{0:T(128)}, f32[2,1,512,256]{3,2,1,0:T(8,128)}, /*index=5*/...) while((s32[]{:T(128)}, f32[1,256,256]{2,1,0:T(8,128)S(1)}, ...), condition=%wide.region_8.9_spmd.clone, body=%wide.region_1.8_spmd.clone.sunk | while | flops 744825600 | bytes 5600154 | solution.py:163
  25.1 0.6 slice.74
  25.7 1.3 fusion.173
  28.3 0.7 subtract_exponential_fusion.3
  29.3 0.4 fusion.176
  30.4 1.3 fusion.179
  33.1 0.6 slice.74
  33.7 1.3 fusion.173
  36.3 0.7 subtract_exponential_fusion.3
  37.2 0.4 fusion.176
  38.3 1.3 fusion.179
  40.5 0.9 pad_maximum_fusion
  41.5 1.3 broadcast_in_dim.51
  42.8 11.9 %all-to-all-start = ((f32[32,1,1]{2,1,0:T(1,128)}), f32[32,1,1]{2,1,0:T(1,128)S(1)}, u32[]{:S(2)}, u32[]{:S(2)}) async-start(f32[32,1,1]{2,1,0:T(1,128)} %broadcast_in_dim.51), calls=%async_computation | async-start | bytes 32768 | tf_op jit(solution)/shard_map/all_to_all | solution.py:30
  54.7 3.5 %convolution_convert_fusion.3 = bf16[1024,128]{1,0:T(8,128)(2,1)S(1)} fusion(bf16[1024,2048]{1,0:T(8,128)(2,1)} %copy-done.1, bf16[2048,128]{1,0:T(8,128)(2,1)} %param.37), kind=kOutput, calls=%fused_computation.91 | convolution fusion | flops 537001984 | bytes 4980736 | tf_op jit(solution)/shard_map/dot_general | solution.py:218
  58.3 3.1 %collective-permute-start = (bf16[256,128]{1,0:T(8,128)(2,1)S(1)}, bf16[256,128]{1,0:T(8,128)(2,1)S(1)}, u32[]{:S(2)}, u32[]{:S(2)}) collective-permute-start(bf16[256,128]{1,0:T(8,128)(2,1)S(1)} %slice.50), channel_id=1, source_target_pairs={{0,8},{8,16},{16,24},{24,32},{32,40},{40,48},{48,56},{56,64},{64,7... | collective-permute-start | bytes 196616 | tf_op jit(solution)/shard_map/ppermute | solution.py:47
  62.2 1.4 copy.90
  63.6 40.4 %all_gather.7 = f32[1,256,257]{2,1,0:T(8,128)S(1)} all-gather(f32[1,8,257]{2,1,0:T(8,128)S(1)} %pad_maximum_fusion.1), channel_id=1, replica_groups=mesh['sp'=32,'tp'=8] {'sp'}, dimensions={1}, use_global_device_ids=true | all-gather | bytes 271392 | tf_op jit(solution)/shard_map/all_gather | solution.py:20
  104.0 3.9 %fusion.128 = f32[1024,128]{0,1:T(8,128)S(1)} fusion(bf16[1024,2048]{1,0:T(8,128)(2,1)} %copy-done.1, bf16[2048,128]{1,0:T(8,128)(2,1)} %param.38), kind=kOutput, calls=%fused_computation.170 | convolution fusion | flops 536870912 | bytes 5242880 | tf_op jit(solution)/shard_map/dot_general | solution.py:243
  107.9 0.8 dynamic_slice.44
  108.7 0.8 dynamic_slice.42
  109.7 0.6 select_reduce_fusion.2
  110.3 2.4 fusion.78
  112.8 5.5 %fusion.60 = f32[1024,2048]{1,0:T(8,128)} fusion(bf16[128,2048]{1,0:T(8,128)(2,1)S(1)} %copy-done.5, bf16[1024,128]{1,0:T(8,128)(2,1)S(1)} %fusion.78, f32[1024,128]{0,1:T(8,128)S(1)} %fusion.128, f32[128]{0:T(128)S(1)} %dynamic_slice.44, bf16[8,128,128]{2,1,0:T(8,128)(2,1)} %param.39, s32[]{:T(128)S(6)} %select_n.99), kind=kOutput, calls=%fused_computation.92 | convolution fusion | flops 571342848 | bytes 9732612 | tf_op jit(solution)/shard_map/dot_general | solution.py:255
  118.3 25.0 %all-gather.2.cloned.1.call-done = f32[32,1,65793]{2,1,0:T(1,128)} async-done(((f32[1,1,65793]{2,1,0:T(1,128)}), f32[32,1,65793]{2,1,0:T(1,128)}) %all-gather.2.cloned.1.call-update) | async-done | bytes 8421520 | tf_op jit(solution)/shard_map/all_gather | solution.py:20
  143.2 1.7 fusion.124
  144.9 0.6 fusion.117
  147.5 26.5 %slice_reduce_fusion.1 = f32[32,65536]{1,0:T(8,128)} fusion(f32[32,1,65793]{2,1,0:T(1,128)} %all-gather.2.cloned.1.call-done), kind=kLoop, calls=%fused_computation.70 | loop fusion | bytes 16777216 | tf_op jit(solution)/shard_map/slice | solution.py:22
  174.0 6.5 %fusion.44 = f32[1,256,256]{2,0,1:T(1,128)S(1)} fusion(f32[4,256,8,256]{3,2,1,0:T(8,128)} %bitcast.314, f32[32]{0:T(128)S(1)} %select_reduce_fusion.1), kind=kOutput, calls=%fused_computation.67 | convolution fusion | flops 25165824 | bytes 8650880 | tf_op jit(solution)/shard_map/kh,khij->hij/dot_general | solution.py:190
  180.8 0.5 fusion.127
  181.4 1.8 multiply_reduce_fusion
  183.3 13.4 %psum.7 = f32[1024]{0:T(1024)S(1)} all-reduce(f32[1024]{0:T(1024)S(1)} %get-tuple-element.219), channel_id=1, replica_groups=mesh['sp'=32,'tp'=8] {'tp'}, use_global_device_ids=true, to_apply=%region_16.17 | all-reduce | flops 1024 | bytes 8192 | tf_op jit(solution)/shard_map/psum | solution.py:210
  196.6 9.6 %add_convert_fusion = bf16[1024,2048]{1,0:T(8,128)(2,1)} fusion(f32[1024,2048]{1,0:T(8,128)} %fusion.60, bf16[256,2048]{1,0:T(8,128)(2,1)S(1)} %copy-done, bf16[1024,2048]{1,0:T(8,128)(2,1)} %copy-done.1, bf16[2048,256]{1,0:T(8,128)(2,1)S(1)} %copy-done.2, f32[1024,256]{0,1:T(8,128)} %get-tuple-element.220, f32[256]{0:T(256)S(1)} %dynamic_slice.42, ...), kind=kOutput, calls=%fused_computation.71 | convolution fusion | flops 2153775104 | bytes 19928064 | tf_op jit(solution)/shard_map/hte,hed->td/dot_general | solution.py:251
  206.2 34.4 %reduce-scatter.2.cloned.1.call-done = bf16[128,2048]{1,0:T(8,128)(2,1)} async-done(((bf16[1024,2048]{1,0:T(8,128)(2,1)}), bf16[128,2048]{1,0:T(8,128)(2,1)}) %reduce-scatter.2.cloned.1.call-update) | async-done | bytes 524304 | tf_op jit(solution)/shard_map/reduce_scatter | solution.py:254
  240.6 1.2 fusion.61
  241.8 2.0 fusion.63
  (101 shorter events, 6.4 us)
Async XLA Ops:
  6.5 190.1 %copy-start = (bf16[256,2048]{1,0:T(8,128)(2,1)S(1)}, bf16[256,2048]{1,0:T(8,128)(2,1)}, u32[]{:S(2)}) copy-start(bf16[256,2048]{1,0:T(8,128)(2,1)} %param.41) | copy-start | bytes 3145732
  6.5 3.2 %copy-start.7 = (f32[2048]{0:T(1024)S(1)}, f32[2048]{0:T(1024)}, u32[]{:S(2)}) copy-start(f32[2048]{0:T(1024)} %param.24) | copy-start | bytes 24580
  6.5 136.7 %all-gather.2.cloned.1.call-start = ((), (), s32[]{:S(2)}) async-start(), calls=%async_computation.2 | async-start | bytes 8701440 | tf_op jit(solution)/shard_map/all_gather | solution.py:20
  9.8 3.2 %copy-start.15 = (f32[8]{0:T(128)S(1)}, f32[8]{0:T(128)}, u32[]{:S(2)}) copy-start(f32[8]{0:T(128)} %param.32) | copy-start | bytes 100
  13.0 8.0 %copy-start.1 = (bf16[1024,2048]{1,0:T(8,128)(2,1)}, bf16[1024,2048]{1,0:T(8,128)(2,1)S(1)}, u32[]{:S(2)}) copy-start(bf16[1024,2048]{1,0:T(8,128)(2,1)S(1)} %fusion.43) | copy-start | bytes 12582916
  13.7 4.0 %copy-start.16 = (f32[8]{0:T(128)S(1)}, f32[8]{0:T(128)}, u32[]{:S(2)}) copy-start(f32[8]{0:T(128)} %param.31) | copy-start | bytes 100
  13.7 4.7 %copy-start.12 = (bf16[2048,256]{1,0:T(8,128)(2,1)S(1)}, bf16[2048,256]{1,0:T(8,128)(2,1)}, u32[]{:S(2)}) copy-start(bf16[2048,256]{1,0:T(8,128)(2,1)} %param.25) | copy-start | bytes 3145732
  17.8 1.9 copy-start.13
  19.7 1.3 copy-start.14
  21.0 1.9 copy-start.10
  40.2 21.2 %copy-start.11 = (f32[1,8]{1,0:T(1,128)S(1)}, f32[1,8]{1,0:T(1,128)}, u32[]{:S(2)}) copy-start(f32[1,8]{1,0:T(1,128)} %param.35) | copy-start | bytes 100
  40.2 21.9 %copy-start.4 = (f32[2,1,512,256]{3,2,1,0:T(8,128)S(1)}, f32[2,1,512,256]{3,2,1,0:T(8,128)}, u32[]{:S(2)}) copy-start(f32[2,1,512,256]{3,2,1,0:T(8,128)} %get-tuple-element.72) | copy-start | bytes 3145732
  42.8 66.7 %all-to-all-start = ((f32[32,1,1]{2,1,0:T(1,128)}), f32[32,1,1]{2,1,0:T(1,128)S(1)}, u32[]{:S(2)}, u32[]{:S(2)}) async-start(f32[32,1,1]{2,1,0:T(1,128)} %broadcast_in_dim.51), calls=%async_computation | async-start | bytes 32768 | tf_op jit(solution)/shard_map/all_to_all | solution.py:30
  54.6 8.9 %copy-start.9 = (f32[1,8,256]{2,1,0:T(8,128)S(1)}, f32[1,8,256]{2,1,0:T(8,128)}, u32[]{:S(2)}) copy-start(f32[1,8,256]{2,1,0:T(8,128)} %param.34) | copy-start | bytes 24580
  54.6 185.9 %reduce-scatter.2.cloned.1.call-start = ((), (), s32[]{:S(2)}) async-start(), calls=%async_computation.3 | async-start | bytes 4718592 | tf_op jit(solution)/shard_map/reduce_scatter | solution.py:254
  58.2 5.3 %copy-start.6 = (bf16[1024,128]{1,0:T(8,128)(2,1)}, bf16[1024,128]{1,0:T(8,128)(2,1)S(1)}, u32[]{:S(2)}) copy-start(bf16[1024,128]{1,0:T(8,128)(2,1)S(1)} %convolution_convert_fusion.3) | copy-start | bytes 786436
  58.3 52.1 %collective-permute-start = (bf16[256,128]{1,0:T(8,128)(2,1)S(1)}, bf16[256,128]{1,0:T(8,128)(2,1)S(1)}, u32[]{:S(2)}, u32[]{:S(2)}) collective-permute-start(bf16[256,128]{1,0:T(8,128)(2,1)S(1)} %slice.50), channel_id=1, source_target_pairs={{0,8},{8,16},{16,24},{24,32},{32,40},{40,48},{48,56},{56,64},{64,7... | collective-permute-start | bytes 196616 | tf_op jit(solution)/shard_map/ppermute | solution.py:47
  107.9 4.8 %copy-start.5 = (bf16[128,2048]{1,0:T(8,128)(2,1)S(1)}, bf16[128,2048]{1,0:T(8,128)(2,1)}, u32[]{:S(2)}) copy-start(bf16[128,2048]{1,0:T(8,128)(2,1)} %param.42) | copy-start | bytes 1572868
  174.0 6.5 %slice-start = ((f32[32,1,65793]{2,1,0:T(1,128)}), f32[32,1,256]{2,1,0:T(1,128)S(1)}, s32[]{:S(2)}) async-start(f32[32,1,65793]{2,1,0:T(1,128)} %all-gather.2.cloned.1.call-done), calls=%async_computation.4 | async-start | bytes 65536 | tf_op jit(solution)/shard_map/slice | solution.py:22
  174.0 7.4 %copy-start.3 = (f32[1024,256]{0,1:T(8,128)S(1)}, f32[1024,256]{0,1:T(8,128)}, u32[]{:S(2)}) copy-start(f32[1024,256]{0,1:T(8,128)} %copy.90) | copy-start | bytes 3145732
  180.5 16.2 %copy-start.2 = (bf16[2048,256]{1,0:T(8,128)(2,1)S(1)}, bf16[2048,256]{1,0:T(8,128)(2,1)}, u32[]{:S(2)}) copy-start(bf16[2048,256]{1,0:T(8,128)(2,1)} %param.28) | copy-start | bytes 3145732
  206.2 35.6 %copy-start.8 = (f32[2048]{0:T(1024)S(1)}, f32[2048]{0:T(1024)}, u32[]{:S(2)}) copy-start(f32[2048]{0:T(1024)} %param.43) | copy-start | bytes 24580
Sparse Core Ops, SparseCore 0:
  41.6 101.5 all-gather.1
  206.4 34.1 reduce-scatter.1
where the time goes:
time: 253 us; the launch traced here: 251 us
  waiting for transfers between devices  59.3 us (23%)
  blocking collectives  53.8 us (21%)
  matrix products  47.1 us (19%)
  local copies, waits for them, and re-layouts  34.6 us (14%)
  other arithmetic  22.3 us (9%)
  between operations  15.8 us (6%)
  starting transfers between devices  15 us (6%)
  loops' own time  2.76 us (1%)
    all_gather x1, blocking collectives, sent_together(): lax.all_gather(both, axis, axis=dim, tiled=True)  40.4 us
    reduce_scatter x1, waiting for transfers between devices, body(): lax.psum_scatter((memory_term + jnp.dot(pool_out, w_out_pool, preferred_e...  34.4 us
    slice x3, local copies, waits for them, and re-layouts, sent_together(): slab = result[..., at:at + column.shape[along]]  26.5 us
    all_gather x1, waiting for transfers between devices, sent_together(): lax.all_gather(both, axis, axis=dim, tiled=True)  25 us
    psum x1, blocking collectives, body(): all_squares = lax.psum(local_squares, 'tp')  13.4 us
    all_to_all x1, starting transfers between devices, sent_to_all(): return lax.all_to_all(copies, axis, split_axis=0, concat_axis=0, tiled=True)  11.9 us
    dot_general x1, matrix products, body(): jnp.einsum('hte,hed->td', memory_out, out_memory, preferred_element_type=...  9.56 us
    dot_general x1, matrix products, body(): jnp.einsum('kh,khij->hij', piece_weight, piece_state, precision=lax.Preci...  6.46 us
  transfers between devices with their start and end apart: 4, of which 2 were waited for; matrix products, arithmetic and copies ran while one was open for 8% of the time, Pallas kernels for 0%

commit v1 on v0

v1 whole, which is shorter than its diff:
```python
import jax
import jax.numpy as jnp
from jax import lax
from jax.experimental import pallas as pl
from jax.experimental.pallas import tpu as pltpu
from jax.sharding import PartitionSpec as P

EPS = 1e-6
NEG = -1e30
F32 = jnp.float32
BF16 = jnp.bfloat16
MESH = pl.DeviceIdType.MESH

T = 1024
D = 2048
H = 256
G = 128
NSP = 32
NZ, NX = 8, 4
NTP = 8
NY = 4
HALO = 256


def nn(a, b):
    return jnp.dot(a, b, preferred_element_type=F32)


def nt(a, b):
    return lax.dot_general(a, b, (((1,), (1,)), ((), ())), preferred_element_type=F32)


def tn(a, b):
    return lax.dot_general(a, b, (((0,), (0,)), ((), ())), preferred_element_type=F32)


def silu(x):
    return x / (1.0 + jnp.exp(-x))


def scan_packed(x, combine, fill):
    lane = lax.broadcasted_iota(jnp.int32, (8, 128), 1)
    sub = lax.broadcasted_iota(jnp.int32, (8, 128), 0)
    for step in (1, 2, 4, 8, 16, 32, 64):
        x = combine(x, jnp.where(lane >= step, pltpu.roll(x, step, 1), fill))
    rows = jnp.broadcast_to(x[:, 127:128], (8, 128))
    before = jnp.where(sub >= 1, pltpu.roll(rows, 1, 0), fill)
    for step in (1, 2, 4):
        before = combine(before, jnp.where(sub >= step, pltpu.roll(before, step, 0), fill))
    return combine(x, before)


def columns_of(packed):
    rows = jnp.concatenate(packed + [jnp.zeros((128 - 8 * len(packed), 128), F32)], axis=0)
    return rows.T


def kernel(
    tokens, pre_gain, w_query, w_key, w_value, w_gate, w_in, w_forget, in_bias, forget_bias, extra, init_memory,
    init_normal, memory_gain, w_pool_in, w_pool_gate, pool_mix, pool_gain, w_out_memory, w_out_pool, post_gain,
    out,
    tok, nrm, wq, wk, wv, wg, wp, gw, pre, bias_i, bias_f, fex, im, inn, mg, pm, pg, wom, wop, post,
    gz, q, k, v, gate, pool_ext, pgate, num, den, cols,
    ustate, usend, urecv, bsend, brecv, ssend, srecv, smat,
    sqs, sqr, zbuf, zsib, part, fwd, r1, r2, r3, r4, r5, r6, obuf,
    lsem, tsem, osem, wsend, wrecv, usem, bsem, hsem, ssem, qsem, zsem, rsend, rrecv,
):
    sp = lax.axis_index("sp")
    tp = lax.axis_index("tp")
    z, x = sp // NX, sp % NX
    y, c = tp // 2, tp % 2
    sib = {"sp": sp, "tp": 2 * y + (1 - c)}
    up = {"sp": sp, "tp": 2 * lax.rem(y + 1, NY) + c}
    down = {"sp": sp, "tp": 2 * lax.rem(y + NY - 1, NY) + c}

    def sp_peer(n):
        kz = n // NX
        dz = lax.rem(4 + (kz + 1) // 2 * (1 - 2 * lax.rem(kz, 2)) + NZ, NZ)
        dx = lax.rem(2 + lax.rem(n, NX), NX)
        dx = jnp.where(lax.rem(n, NX) == 1, 1, jnp.where(lax.rem(n, NX) == 2, 3, jnp.where(lax.rem(n, NX) == 3, 0, 2)))
        return lax.rem(z + dz, NZ) * NX + lax.rem(x + dx, NX)

    barrier = pltpu.get_barrier_semaphore()

    def greet_sp(n, carry):
        pl.semaphore_signal(barrier, inc=1, device_id={"sp": sp_peer(n), "tp": tp}, device_id_type=MESH)
        return carry

    def greet_tp(n, carry):
        pl.semaphore_signal(barrier, inc=1, device_id={"sp": sp, "tp": lax.rem(tp + n, NTP)}, device_id_type=MESH)
        return carry

    lax.fori_loop(0, NSP - 1, greet_sp, 0)
    lax.fori_loop(1, NTP, greet_tp, 0)

    tok_copies = [
        pltpu.make_async_copy(tokens.at[pl.ds(256 * i, 256)], tok.at[pl.ds(256 * i, 256)], tsem.at[i]) for i in range(4)
    ]
    loads = [
        (pre_gain, pre), (w_key, wk), (w_value, wv), (w_in, gw.at[pl.ds(0, 8)]), (w_forget, gw.at[pl.ds(8, 8)]),
        (in_bias, bias_i), (forget_bias, bias_f), (extra, fex), (init_memory, im), (init_normal, inn),
        (w_query, wq), (w_gate, wg), (w_pool_in, wp.at[:, pl.ds(0, G)]), (w_pool_gate, wp.at[:, pl.ds(G, G)]),
        (memory_gain.at[:, pl.ds(pl.multiple_of(tp * H, H), H)], mg), (pool_mix.at[tp], pm),
        (pool_gain.at[:, pl.ds(pl.multiple_of(tp * G, G), G)], pg),
        (w_out_memory, wom.at[pl.ds(0, H)]), (w_out_pool, wop.at[pl.ds(0, G)]), (post_gain, post),
    ]
    copies = [pltpu.make_async_copy(src, dst, lsem.at[i]) for i, (src, dst) in enumerate(loads)]
    gw[16:128, :] = jnp.zeros((112, D), BF16)
    copies[0].start()
    for copy in tok_copies:
        copy.start()
    for copy in copies[1:]:
        copy.start()

    def norm_rows(i):
        tok_copies[i].wait()
        rows = pl.ds(256 * i, 256)
        total = jnp.zeros((256, 128), F32)
        for col in range(D // 128):
            piece = tok[rows, pl.ds(128 * col, 128)].astype(F32)
            total = total + piece * piece
        scale = lax.rsqrt(jnp.sum(total, axis=1, keepdims=True) / D + EPS)
        for col in range(D // 128):
            at = pl.ds(128 * col, 128)
            piece = tok[rows, at].astype(F32)
            nrm[rows, at] = (piece * scale * pre[:, at]).astype(BF16)

    copies[0].wait()
    norm_rows(0)
    for i in range(1, 5):
        copies[i].wait()
    for i in range(4):
        if i < 3:
            norm_rows(i + 1)
        rows = pl.ds(256 * i, 256)
        normed = nrm[rows, :]
        k[rows, :] = nn(normed, wk[...]).astype(BF16)
        v[rows, :] = nn(normed, wv[...]).astype(BF16)
        gz[rows, :] = nt(normed, gw[...])
    for i in range(5, 10):
        copies[i].wait()

    head8 = lax.broadcasted_iota(jnp.int32, (8, 128), 0) == tp
    lin, lfor = [], []
    for r in range(8):
        block = gz[pl.ds(128 * r, 128), :].T
        lin.append(jnp.sum(jnp.where(head8, block[0:8], 0.0), axis=0, keepdims=True))
        lfor.append(jnp.sum(jnp.where(head8, block[8:16], 0.0), axis=0, keepdims=True))
    own8 = lax.broadcasted_iota(jnp.int32, (1, 8), 1) == tp
    shift_i = jnp.sum(jnp.where(own8, bias_i[...], 0.0), axis=1, keepdims=True)
    shift_f = jnp.sum(jnp.where(own8, bias_f[...], 0.0), axis=1, keepdims=True)
    log_input = jnp.concatenate(lin, axis=0) + shift_i
    pre_keep = jnp.concatenate(lfor, axis=0) + shift_f
    log_keep = jnp.minimum(pre_keep, 0.0) - jnp.log1p(jnp.exp(-jnp.abs(pre_keep))) + fex[...]
    keep_run = scan_packed(log_keep, jnp.add, 0.0)
    offer = log_input - keep_run
    best = scan_packed(offer, jnp.maximum, NEG)
    keep_all = keep_run[7:8, 127:128]
    best_all = best[7:8, 127:128]
    write = jnp.exp(offer - best_all)
    colA = columns_of([write, best])

    def column(source, index, i):
        at = 8 * index + 2 * i
        return jnp.concatenate([source[:, at : at + 1], source[:, at + 1 : at + 2]], axis=0)

    state = jnp.zeros((H, H), F32)
    normal = jnp.zeros((1, H), F32)
    for i in range(4):
        rows = pl.ds(256 * i, 256)
        weighted = column(colA, 0, i) * k[rows, :].astype(F32)
        normal = normal + jnp.sum(weighted, axis=0, keepdims=True)
        state = state + tn(weighted.astype(BF16), v[rows, :])
    ustate[...] = state
    lane128 = lax.broadcasted_iota(jnp.int32, (1, 128), 1)
    bsend[0:1, :] = normal[:, 0:128]
    bsend[1:2, :] = normal[:, 128:256]
    bsend[2:3, :] = jnp.where(lane128 < 64, keep_all + best_all, keep_all)
    placed = jnp.concatenate([inn[...], jnp.zeros((1, 120), F32)], axis=1)
    bsend[3:4, :] = pltpu.roll(placed, 8 * lax.rem(sp, 16), 1)

    def pack_slab(j, carry):
        slab = ustate[pl.ds(pl.multiple_of(8 * j, 8), 8), :]
        usend[j] = jnp.concatenate([slab[:, 0:128], slab[:, 128:256]], axis=0).astype(BF16)
        return carry

    lax.fori_loop(0, NSP, pack_slab, 0)
    urecv[sp] = usend[sp]
    brecv[sp] = bsend[...]

    pl.semaphore_wait(barrier, NSP - 1 + NTP - 1)

    def b_copy(dst):
        return pltpu.make_async_remote_copy(
            src_ref=bsend, dst_ref=brecv.at[sp], send_sem=bsem.at[0], recv_sem=bsem.at[1],
            device_id={"sp": dst, "tp": tp}, device_id_type=MESH,
        )

    def u_copy(dst):
        return pltpu.make_async_remote_copy(
            src_ref=usend.at[dst], dst_ref=urecv.at[sp], send_sem=usem.at[0], recv_sem=usem.at[1],
            device_id={"sp": dst, "tp": tp}, device_id_type=MESH,
        )

    def s_copy(dst):
        return pltpu.make_async_remote_copy(
            src_ref=ssend.at[dst], dst_ref=srecv.at[sp], send_sem=ssem.at[0], recv_sem=ssem.at[1],
            device_id={"sp": dst, "tp": tp}, device_id_type=MESH,
        )

    def send_first(n, carry):
        dst = sp_peer(n)
        b_copy(dst).start()
        u_copy(dst).start()
        return carry

    def send_second(n, carry):
        s_copy(sp_peer(n)).start()
        return carry

    lax.fori_loop(0, NSP - 1, send_first, 0)
    w_copies = [
        pltpu.make_async_remote_copy(
            src_ref=src, dst_ref=dst, send_sem=wsend.at[i], recv_sem=wrecv.at[i], device_id=sib, device_id_type=MESH
        )
        for i, (src, dst) in enumerate([(w_out_memory, wom.at[pl.ds(H, H)]), (w_out_pool, wop.at[pl.ds(G, G)])])
    ]
    for copy in w_copies:
        copy.start()

    for i in range(10, 18):
        copies[i - 0].wait() if i < 17 else None
    for i in range(4):
        rows = pl.ds(256 * i, 256)
        both = nn(nrm[rows, :], wp[...])
        pool_ext[pl.ds(HALO + 256 * i, 256), :] = both[:, 0:G].astype(BF16)
        pgate[rows, :] = silu(both[:, G : 2 * G]) * pg[...]
    halo = pltpu.make_async_remote_copy(
        src_ref=pool_ext.at[pl.ds(T, HALO)], dst_ref=pool_ext.at[pl.ds(0, HALO)], send_sem=hsem.at[0],
        recv_sem=hsem.at[1], device_id={"sp": lax.rem(sp + 1, NSP), "tp": tp}, device_id_type=MESH,
    )
    halo.start()
    for i in range(4):
        rows = pl.ds(256 * i, 256)
        q[rows, :] = nn(nrm[rows, :], wq[...]).astype(BF16)

    head_scale = H ** (-0.5)
    for i in range(4):
        rows = pl.ds(256 * i, 256)
        length = 256 * (i + 1)
        scores = nt(q[rows, :], k[pl.ds(0, length), :])
        source = jnp.concatenate([offer[r : r + 1, :] for r in range(2 * (i + 1))], axis=1)
        exponent = source - column(colA, 1, i)
        ahead = lax.broadcasted_iota(jnp.int32, (256, length), 1) > lax.broadcasted_iota(
            jnp.int32, (256, length), 0
        ) + 256 * i
        weights = jnp.exp(jnp.where(ahead, NEG, exponent)) * scores * head_scale
        den[rows, :] = jnp.broadcast_to(jnp.sum(weights, axis=1, keepdims=True), (256, 128))
        num[rows, :] = nn(weights.astype(BF16), v[pl.ds(0, length), :])
    for i in range(4):
        rows = pl.ds(256 * i, 256)
        gate[rows, :] = silu(nn(nrm[rows, :], wg[...])) * mg[...]

    pltpu.make_async_copy(brecv.at[pl.ds(0, NSP - 1)], brecv.at[pl.ds(0, NSP - 1)], bsem.at[1]).wait()
    pltpu.make_async_copy(urecv.at[pl.ds(0, NSP - 1)], urecv.at[pl.ds(0, NSP - 1)], usem.at[1]).wait()
    memory = jnp.concatenate([im[:, 0:128], im[:, 128:256]], axis=0)
    start_low = jnp.zeros((1, 128), F32)
    start_high = jnp.zeros((1, 128), F32)
    for j in range(16):
        start_low = start_low + brecv[j, 3:4, :]
        start_high = start_high + brecv[16 + j, 3:4, :]
    carried_n = jnp.concatenate([start_low, start_high], axis=0)
    stab = jnp.zeros((1, 1), F32)
    my_stab = jnp.zeros((1, 1), F32)
    my_n = carried_n
    for j in range(NSP):
        mine = sp == j
        my_stab = jnp.where(mine, stab, my_stab)
        my_n = jnp.where(mine, carried_n, my_n)
        ssend[j] = memory.astype(BF16)
        if j < NSP - 1:
            piece_stab = brecv[j, 2:3, 0:1]
            piece_keep = brecv[j, 2:3, 64:65]
            new_stab = jnp.maximum(stab + piece_keep, piece_stab)
            fade = jnp.exp(stab + piece_keep - new_stab)
            weight = jnp.exp(piece_stab - new_stab)
            memory = fade * memory + weight * urecv[j].astype(F32)
            carried_n = fade * carried_n + weight * brecv[j, 0:2, :]
            stab = new_stab
    srecv[sp] = ssend[sp]
    lax.fori_loop(0, NSP - 1, send_second, 0)

    joint = jnp.maximum(best, my_stab)
    local_weight = jnp.exp(best - joint)
    carry_weight = jnp.exp(my_stab - joint) * head_scale
    least = jnp.exp(-(keep_run + joint))
    cols[...] = columns_of([local_weight, carry_weight, least])
    n_row = jnp.concatenate([my_n[0:1, :], my_n[1:2, :]], axis=1)
    colB = cols[...]
    for i in range(4):
        rows = pl.ds(256 * i, 256)
        carried = jnp.sum(q[rows, :].astype(F32) * n_row, axis=1, keepdims=True)
        full = den[rows, 0:1] * column(colB, 0, i) + column(colB, 1, i) * carried
        inverse = 1.0 / jnp.maximum(jnp.abs(full), column(colB, 2, i))
        num[rows, :] = num[rows, :] * (column(colB, 0, i) * inverse)
        den[rows, :] = jnp.broadcast_to(column(colB, 1, i) * inverse, (256, 128))

    halo.wait_recv()
    first = jnp.where(sp == 0, 0.0, 1.0)
    pool_ext[pl.ds(0, HALO), :] = (pool_ext[pl.ds(0, HALO), :].astype(F32) * first).astype(BF16)
    window = lax.shift_left(jnp.int32(2), tp)
    for i in range(4):
        rows = pl.ds(256 * i, 256)
        near = pool_ext[pl.ds(256 * i, 512), :]
        target = lax.broadcasted_iota(jnp.int32, (256, 512), 0) + HALO
        back = target - lax.broadcasted_iota(jnp.int32, (256, 512), 1)
        band = jnp.where((back >= 0) & (back < window), 1.0, 0.0).astype(BF16)
        sums = nn(band, near)
        place = sp * T + 256 * i + lax.broadcasted_iota(jnp.int32, (256, 1), 0) + 1
        count = jnp.minimum(place, window).astype(F32)
        pooled = (sums / count - near[HALO:, :].astype(F32)).astype(BF16)
        mixed = nn(pooled, pm[...]) * pgate[rows, :]
        zbuf[2 * i, :, H : H + G] = mixed[0:128].astype(BF16)
        zbuf[2 * i + 1, :, H : H + G] = mixed[128:256].astype(BF16)
    for i in range(17, 20):
        copies[i].wait()

    pltpu.make_async_copy(srecv.at[pl.ds(0, NSP - 1)], srecv.at[pl.ds(0, NSP - 1)], ssem.at[1]).wait()
    for j in range(NSP):
        slab = srecv[j].astype(F32)
        smat[8 * j : 8 * j + 8, 0:128] = slab[0:8]
        smat[8 * j : 8 * j + 8, 128:256] = slab[8:16]
    held = smat[...].astype(BF16)
    lane_sq = lax.broadcasted_iota(jnp.int32, (128, 128), 1)
    squares = jnp.zeros((128, 128), F32)
    for i in range(4):
        rows = pl.ds(256 * i, 256)
        memory_rows = num[rows, :] + den[rows, 0:1] * nn(q[rows, :], held)
        sq = jnp.sum(memory_rows * memory_rows, axis=1, keepdims=True)
        squares = jnp.where(lane_sq == 2 * i, sq[0:128], squares)
        squares = jnp.where(lane_sq == 2 * i + 1, sq[128:256], squares)
        gated = (memory_rows * gate[rows, :]).astype(BF16)
        zbuf[2 * i, :, 0:H] = gated[0:128]
        zbuf[2 * i + 1, :, 0:H] = gated[128:256]
    own_sq = squares.T[0:8]
    sqs[...] = own_sq

    def sq_copy(n):
        return pltpu.make_async_remote_copy(
            src_ref=sqs, dst_ref=sqr.at[n], send_sem=qsem.at[0], recv_sem=qsem.at[1],
            device_id={"sp": sp, "tp": lax.rem(tp + n + 1, NTP)}, device_id_type=MESH,
        )

    def z_copy(n):
        return pltpu.make_async_remote_copy(
            src_ref=zbuf.at[2 * n + 1 - c], dst_ref=zsib.at[n], send_sem=zsem.at[0], recv_sem=zsem.at[1],
            device_id=sib, device_id_type=MESH,
        )

    for n in range(NTP - 1):
        sq_copy(n).start()
    for n in range(NY):
        z_copy(n).start()
    for copy in w_copies:
        copy.wait_recv()
    pltpu.make_async_copy(zsib, zsib, zsem.at[1]).wait()
    pltpu.make_async_copy(sqr, sqr, qsem.at[1]).wait()
    total = own_sq
    for n in range(NTP - 1):
        total = total + sqr[n]
    sqs_scale = lax.rsqrt(total / (NTP * H) + EPS)
    cols[0:8, :] = sqs_scale
    eye = lax.broadcasted_iota(jnp.int32, (128, 128), 0) == lax.broadcasted_iota(jnp.int32, (128, 128), 1)

    def out_block(dy):
        to = lax.rem(y + dy, NY)
        mine, other = zbuf[2 * to + c], zsib[to]
        row = cols[pl.ds(2 * to + c, 1), :]
        scale = jnp.sum(jnp.where(eye, jnp.broadcast_to(row, (128, 128)), 0.0), axis=1, keepdims=True)
        memory_in = jnp.concatenate([mine[:, 0:H], other[:, 0:H]], axis=1)
        pool_in = jnp.concatenate([mine[:, H:], other[:, H:]], axis=1)
        for half in range(2):
            for quarter in range(2):
                at = pl.ds(1024 * half + 512 * quarter, 512)
                term = nn(memory_in, wom[:, at]) * scale + nn(pool_in, wop[:, at])
                part[dy, half, :, pl.ds(512 * quarter, 512)] = term.astype(BF16)

    def rs_copy(n, src, dst, to):
        return pltpu.make_async_remote_copy(
            src_ref=src, dst_ref=dst, send_sem=rsend.at[n], recv_sem=rrecv.at[n], device_id=to, device_id_type=MESH
        )

    rs = [
        rs_copy(0, part.at[2, 0], r1, up), rs_copy(1, part.at[2, 1], r2, down),
        rs_copy(2, part.at[1, 1], r3, up), rs_copy(3, part.at[3, 0], r4, down),
        rs_copy(4, fwd.at[0], r5, up), rs_copy(5, fwd.at[1], r6, down),
    ]
    out_block(2)
    rs[0].start()
    rs[1].start()
    out_block(1)
    rs[2].start()
    out_block(3)
    rs[3].start()
    out_block(0)
    rs[0].wait_recv()
    fwd[0] = (part[1, 0].astype(F32) + r1[...].astype(F32)).astype(BF16)
    rs[4].start()
    rs[1].wait_recv()
    fwd[1] = (part[3, 1].astype(F32) + r2[...].astype(F32)).astype(BF16)
    rs[5].start()
    for n in range(2, 6):
        rs[n].wait_recv()
    low = part[0, 0].astype(F32) + r4[...].astype(F32) + r5[...].astype(F32)
    high = part[0, 1].astype(F32) + r3[...].astype(F32) + r6[...].astype(F32)
    mean = (jnp.sum(low * low, axis=1, keepdims=True) + jnp.sum(high * high, axis=1, keepdims=True)) / D
    scale = lax.rsqrt(mean + EPS)
    obuf[:, 0:1024] = (low * scale * post[:, 0:1024]).astype(BF16)
    obuf[:, 1024:2048] = (high * scale * post[:, 1024:2048]).astype(BF16)
    finish = pltpu.make_async_copy(obuf, out, osem.at[0])
    finish.start()

    def drain_first(n, carry):
        b_copy(sp_peer(n)).wait_send()
        u_copy(sp_peer(n)).wait_send()
        s_copy(sp_peer(n)).wait_send()
        return carry

    lax.fori_loop(0, NSP - 1, drain_first, 0)
    for copy in w_copies:
        copy.wait_send()
    halo.wait_send()
    for n in range(NTP - 1):
        sq_copy(n).wait_send()
    for n in range(NY):
        z_copy(n).wait_send()
    for copy in rs:
        copy.wait_send()
    finish.wait()


def body(
    tokens, pre_gain, w_query, w_key, w_value, memory_output_gate_weight, w_input_gate, w_forget_gate, input_bias,
    forget_bias, forget_extra, initial_memory, initial_normal, memory_gain, w_pool_input, w_pool_gate, pool_mix,
    pool_gain, w_out_memory, w_out_pool, post_gain,
):
    args = (
        tokens, pre_gain.reshape(1, D), w_query, w_key, w_value, memory_output_gate_weight, w_input_gate.T,
        w_forget_gate.T, input_bias.reshape(1, 8), forget_bias.reshape(1, 8), forget_extra.reshape(8, 128),
        initial_memory.reshape(8, H), initial_normal, memory_gain.reshape(1, D), w_pool_input, w_pool_gate, pool_mix,
        pool_gain.reshape(1, NTP * G), w_out_memory, w_out_pool, post_gain.reshape(1, D),
    )
    vmem = pltpu.VMEM
    dma = pltpu.SemaphoreType.DMA
    scratch = [
        vmem((T, D), BF16), vmem((T, D), BF16), vmem((D, H), BF16), vmem((D, H), BF16), vmem((D, H), BF16),
        vmem((D, H), BF16), vmem((D, 2 * G), BF16), vmem((128, D), BF16), vmem((1, D), F32), vmem((1, 8), F32),
        vmem((1, 8), F32), vmem((8, 128), F32), vmem((8, H), F32), vmem((1, 8), F32), vmem((1, H), F32),
        vmem((G, G), BF16), vmem((1, G), F32), vmem((2 * H, D), BF16), vmem((2 * G, D), BF16), vmem((1, D), F32),
        vmem((T, 128), F32), vmem((T, H), BF16), vmem((T, H), BF16), vmem((T, H), BF16), vmem((T, H), F32),
        vmem((HALO + T, G), BF16), vmem((T, G), F32), vmem((T, H), F32), vmem((T, 128), F32), vmem((128, 128), F32),
        vmem((H, H), F32), vmem((NSP, 16, 128), BF16), vmem((NSP, 16, 128), BF16), vmem((4, 128), F32),
        vmem((NSP, 4, 128), F32), vmem((NSP, 16, 128), BF16), vmem((NSP, 16, 128), BF16), vmem((H, H), F32),
        vmem((8, 128), F32), vmem((NTP - 1, 8, 128), F32), vmem((NTP, 128, H + G), BF16), vmem((NY, 128, H + G), BF16),
        vmem((NY, 2, 128, 1024), BF16), vmem((2, 128, 1024), BF16), vmem((128, 1024), BF16), vmem((128, 1024), BF16),
        vmem((128, 1024), BF16), vmem((128, 1024), BF16), vmem((128, 1024), BF16), vmem((128, 1024), BF16),
        vmem((128, D), BF16),
        dma((20,)), dma((4,)), dma((1,)), dma((2,)), dma((2,)), dma((2,)), dma((2,)), dma((2,)), dma((2,)), dma((2,)),
        dma((2,)), dma((6,)), dma((6,)),
    ]
    anywhere = pl.BlockSpec(memory_space=pl.ANY)
    return pl.pallas_call(
        kernel,
        out_shape=jax.ShapeDtypeStruct((128, D), BF16),
        in_specs=[anywhere] * len(args),
        out_specs=anywhere,
        scratch_shapes=scratch,
        compiler_params=pltpu.CompilerParams(
            collective_id=0, has_side_effects=True, vmem_limit_bytes=60 * 1024 * 1024
        ),
    )(*args)


def solution(mesh):
    in_specs = (
        P("sp", None), P(), P(None, "tp"), P(None, "tp"), P(None, "tp"), P(None, "tp"), P(), P(), P(), P(),
        P("sp", "tp"), P("tp", "sp", None), P("tp", "sp"), P(), P(None, "tp"), P(None, "tp"), P(), P(),
        P("tp", None), P("tp", None), P(),
    )
    return jax.shard_map(
        body, mesh=mesh, in_specs=in_specs, out_specs=P(("sp", "tp"), None), check_vma=False
    )
```

time: 253 us -> 59.8 us (0.24)
  waiting for transfers between devices: 59.3 us -> 0 us
  Pallas kernels: 0 us -> 57.8 us
  blocking collectives: 53.8 us -> 0 us
  matrix products: 47.1 us -> 0 us
  local copies, waits for them, and re-layouts: 34.6 us -> 1.88 us
  other arithmetic: 22.3 us -> 0 us
  between operations: 15.8 us -> 0.01 us
  starting transfers between devices: 15 us -> 0 us
  loops' own time: 2.76 us -> 0 us
    pallas_call x0 -> x1, Pallas kernels: none -> 57.8 us  [body(): pl.pallas_call(kernel, out_shape=jax.ShapeDtypeStruct((128, D), BF16), in...]
    dot_general x24 -> x0, matrix products: 47.1 us -> none  [the longest x1 9.56 us: body(): jnp.einsum('hte,hed->td', memory_out, out_memory, preferred_element_type=...]
    all_gather x1 -> x0, blocking collectives: 40.4 us -> none  [sent_together(): lax.all_gather(both, axis, axis=dim, tiled=True)]
    reduce_scatter x1 -> x0, waiting for transfers between devices: 34.4 us -> none  [body(): lax.psum_scatter((memory_term + jnp.dot(pool_out, w_out_pool, preferred_e...]
    slice x8 -> x0, local copies, waits for them, and re-layouts: 28.1 us -> none  [the longest x3 26.5 us: sent_together(): slab = result[..., at:at + column.shape[along]]]
    all_gather x1 -> x0, waiting for transfers between devices: 25 us -> none  [sent_together(): lax.all_gather(both, axis, axis=dim, tiled=True)]
    psum x1 -> x0, blocking collectives: 13.4 us -> none  [body(): all_squares = lax.psum(local_squares, 'tp')]
    all_to_all x1 -> x0, starting transfers between devices: 11.9 us -> none  [sent_to_all(): return lax.all_to_all(copies, axis, split_axis=0, concat_axis=0, tiled=True)]
  transfers between devices with their start and end apart: 4 -> 0, of which waited for: 2 -> 0; matrix products, arithmetic and copies ran while one was open for 8% -> 0% of each run, Pallas kernels for 0% -> 0%
where the time goes in v1:
time: 59.8 us; the launch traced here: 59.7 us
  Pallas kernels  57.8 us (97%)
  local copies, waits for them, and re-layouts  1.88 us (3%)
    pallas_call x1, Pallas kernels, body(): pl.pallas_call(kernel, out_shape=jax.ShapeDtypeStruct((128, D), BF16), in...  57.8 us
    unnamed x1, local copies, waits for them, and re-layouts  1.88 us

profile of v1, /device:TPU:1, one launch (start us, length us, event | category | flops | bytes accessed | tf_op | source)
XLA Modules:
  0.0 59.7 jit_solution(17035136483859827368)
XLA Ops:
  0.0 57.8 %shard_map.199 = bf16[128,2048]{1,0:T(8,128)(2,1)} custom-call(bf16[1024,2048]{1,0:T(8,128)(2,1)} %tokens.1, f32[1,2048]{1,0:T(1,128)} %bitcast.12, bf16[2048,256]{1,0:T(8,128)(2,1)} %w_query.1, bf16[2048,256]{1,0:T(8,128)(2,1)} %w_key.1, bf16[2048,256]{1,0:T(8,128)(2,1)} %w_value.1, bf16[2048,256]{1,0:T(8,128)(2,1)} %w_gate.1, bf16[8,2048]{1,0:T(8,128)(2,1)} %bitcast.10, ...), custom_call_target="tpu_custom_call" | custom-call | tf_op jit(solution)/shard_map/pallas_call | solution.py:472
  57.8 1.9 %copy.23 = bf16[128,2048]{1,0:T(8,128)(2,1)} copy(bf16[128,2048]{1,0:T(8,128)(2,1)} %shard_map.199) | data formatting | bytes 1048576

commit v2 on v1

v2 whole, which is shorter than its diff:
```python
import jax
import jax.numpy as jnp
from jax import lax
from jax.experimental import pallas as pl
from jax.experimental.pallas import tpu as pltpu
from jax.sharding import PartitionSpec as P

EPS = 1e-6
NEG = -1e30
F32 = jnp.float32
BF16 = jnp.bfloat16
MESH = pl.DeviceIdType.MESH

T = 1024
D = 2048
H = 256
G = 128
NSP = 32
NZ, NX = 8, 4
NTP = 8
NY = 4
HALF = NSP // 2
HALO = 256


def nn(a, b):
    return jnp.dot(a, b, preferred_element_type=F32)


def nt(a, b):
    return lax.dot_general(a, b, (((1,), (1,)), ((), ())), preferred_element_type=F32)


def tn(a, b):
    return lax.dot_general(a, b, (((0,), (0,)), ((), ())), preferred_element_type=F32)


def silu(x):
    return x / (1.0 + jnp.exp(-x))


class Phases:
    scope = None

    def __call__(self, name):
        if self.scope is not None:
            self.scope.__exit__(None, None, None)
        self.scope = jax.named_scope(name) if name else None
        if name:
            self.scope.__enter__()


def scan_packed(x, combine, fill):
    lane = lax.broadcasted_iota(jnp.int32, (8, 128), 1)
    sub = lax.broadcasted_iota(jnp.int32, (8, 128), 0)
    for step in (1, 2, 4, 8, 16, 32, 64):
        x = combine(x, jnp.where(lane >= step, pltpu.roll(x, step, 1), fill))
    rows = jnp.broadcast_to(x[:, 127:128], (8, 128))
    before = jnp.where(sub >= 1, pltpu.roll(rows, 1, 0), fill)
    for step in (1, 2, 4):
        before = combine(before, jnp.where(sub >= step, pltpu.roll(before, step, 0), fill))
    return combine(x, before)


def columns_of(packed):
    rows = jnp.concatenate(packed + [jnp.zeros((128 - 8 * len(packed), 128), F32)], axis=0)
    return rows.T


def kernel(
    tokens, pre_gain, w_query, w_key, w_value, w_gate, w_in, w_forget, in_bias, forget_bias, extra, init_memory,
    init_normal, memory_gain, w_pool_in, w_pool_gate, pool_mix, pool_gain, w_out_memory, w_out_pool, post_gain,
    out,
    tok, nrm, wq, wk, wv, wg, wp, wpg, gw, pre, bias_i, bias_f, fex, im, inn, mg, pm, pg, wom, wop, post,
    gz, q, k, v, gate, pool_ext, pgate, num, den, cols,
    ustate, usend, urecv, bsend, brecv, ssend, srecv, smat,
    sqs, sqr, zbuf, zsib, pbuf, psib, ppart, part, fwd, r1, r2, r3, r4, r5, r6, rp1, rp2,
    lsem, tsem, wsend, wrecv, usem, bsem, hsem, ssem, qsem, zsem, psem, rsend, rrecv,
):
    sp = lax.axis_index("sp")
    tp = lax.axis_index("tp")
    z, x = sp // NX, sp % NX
    y, c = tp // 2, tp % 2
    sib = {"sp": sp, "tp": 2 * y + (1 - c)}
    up = {"sp": sp, "tp": 2 * lax.rem(y + 1, NY) + c}
    down = {"sp": sp, "tp": 2 * lax.rem(y + NY - 1, NY) + c}

    def sp_peer(n):
        kz = n // NX
        dz = lax.rem(4 + (kz + 1) // 2 * (1 - 2 * lax.rem(kz, 2)) + NZ, NZ)
        dx = lax.rem(2 + lax.rem(n, NX), NX)
        dx = jnp.where(lax.rem(n, NX) == 1, 1, jnp.where(lax.rem(n, NX) == 2, 3, jnp.where(lax.rem(n, NX) == 3, 0, 2)))
        return lax.rem(z + dz, NZ) * NX + lax.rem(x + dx, NX)

    phase = Phases()
    phase("loads")
    tok_copies = [
        pltpu.make_async_copy(tokens.at[pl.ds(256 * i, 256)], tok.at[pl.ds(256 * i, 256)], tsem.at[i]) for i in range(4)
    ]
    loads = [
        (pre_gain, pre), (w_in, gw.at[pl.ds(0, 8)]), (w_forget, gw.at[pl.ds(8, 8)]), (w_key, wk),
        (w_pool_in, wp.at[:, pl.ds(0, G)]), (w_value, wv),
        (in_bias, bias_i), (forget_bias, bias_f), (extra, fex), (init_memory, im), (init_normal, inn),
        (w_query, wq), (w_gate, wg), (w_pool_gate, wpg),
        (memory_gain.at[:, pl.ds(pl.multiple_of(tp * H, H), H)], mg), (pool_mix.at[tp], pm),
        (pool_gain.at[:, pl.ds(pl.multiple_of(tp * G, G), G)], pg),
        (w_out_memory, wom.at[pl.ds(0, H)]), (w_out_pool, wop.at[pl.ds(0, G)]), (post_gain, post),
    ]
    copies = [pltpu.make_async_copy(src, dst, lsem.at[i]) for i, (src, dst) in enumerate(loads)]
    tok_copies[0].start()
    for copy in copies[0:3]:
        copy.start()
    tok_copies[1].start()
    copies[3].start()
    copies[4].start()
    tok_copies[2].start()
    tok_copies[3].start()

    phase("greet")
    barrier = pltpu.get_barrier_semaphore()

    def greet_sp(n, carry):
        pl.semaphore_signal(barrier, inc=1, device_id={"sp": sp_peer(n), "tp": tp}, device_id_type=MESH)
        return carry

    def greet_tp(n, carry):
        pl.semaphore_signal(barrier, inc=1, device_id={"sp": sp, "tp": lax.rem(tp + n, NTP)}, device_id_type=MESH)
        return carry

    lax.fori_loop(0, NSP - 1, greet_sp, 0)
    lax.fori_loop(1, NTP, greet_tp, 0)

    def norm_rows(i):
        tok_copies[i].wait()
        rows = pl.ds(256 * i, 256)
        total = jnp.zeros((256, 128), F32)
        for col in range(D // 128):
            piece = tok[rows, pl.ds(128 * col, 128)].astype(F32)
            total = total + piece * piece
        scale = lax.rsqrt(jnp.sum(total, axis=1, keepdims=True) / D + EPS)
        for col in range(D // 128):
            at = pl.ds(128 * col, 128)
            piece = tok[rows, at].astype(F32)
            nrm[rows, at] = (piece * scale * pre[:, at]).astype(BF16)

    phase("gw")
    for i in (0, 1, 2):
        copies[i].wait()
    for col in range(D // 128):
        at = pl.ds(128 * col, 128)
        logits = jnp.concatenate([gw[:, at].astype(F32), jnp.zeros((112, 128), F32)], axis=0)
        wp[at, G : 2 * G] = logits.T.astype(BF16)
    phase("norm0")
    norm_rows(0)
    for copy in copies[5:]:
        copy.start()
    for i in (3, 4):
        copies[i].wait()
    for i in range(4):
        phase("kv%d" % i)
        if i < 3:
            norm_rows(i + 1)
        rows = pl.ds(256 * i, 256)
        normed = nrm[rows, :]
        both = nn(normed, wp[...])
        pool_ext[pl.ds(HALO + 256 * i, 256), :] = both[:, 0:G].astype(BF16)
        gz[rows, :] = both[:, G : 2 * G]
        k[rows, :] = nn(normed, wk[...]).astype(BF16)
    phase("gates")
    for i in range(5, 11):
        copies[i].wait()
    for i in range(2):
        rows = pl.ds(512 * i, 512)
        v[rows, :] = nn(nrm[rows, :], wv[...]).astype(BF16)

    head8 = lax.broadcasted_iota(jnp.int32, (8, 128), 0) == tp
    lin, lfor = [], []
    for r in range(8):
        block = gz[pl.ds(128 * r, 128), :].T
        lin.append(jnp.sum(jnp.where(head8, block[0:8], 0.0), axis=0, keepdims=True))
        lfor.append(jnp.sum(jnp.where(head8, block[8:16], 0.0), axis=0, keepdims=True))
    own8 = lax.broadcasted_iota(jnp.int32, (1, 8), 1) == tp
    shift_i = jnp.sum(jnp.where(own8, bias_i[...], 0.0), axis=1, keepdims=True)
    shift_f = jnp.sum(jnp.where(own8, bias_f[...], 0.0), axis=1, keepdims=True)
    log_input = jnp.concatenate(lin, axis=0) + shift_i
    pre_keep = jnp.concatenate(lfor, axis=0) + shift_f
    log_keep = jnp.minimum(pre_keep, 0.0) - jnp.log1p(jnp.exp(-jnp.abs(pre_keep))) + fex[...]
    keep_run = scan_packed(log_keep, jnp.add, 0.0)
    offer = log_input - keep_run
    best = scan_packed(offer, jnp.maximum, NEG)
    keep_all = keep_run[7:8, 127:128]
    best_all = best[7:8, 127:128]
    write = jnp.exp(offer - best_all)
    colA = columns_of([write, best])

    def column(source, index, i):
        at = 8 * index + 2 * i
        return jnp.concatenate([source[:, at : at + 1], source[:, at + 1 : at + 2]], axis=0)

    phase("state")
    state = jnp.zeros((H, H), F32)
    normal = jnp.zeros((1, H), F32)
    for i in range(4):
        rows = pl.ds(256 * i, 256)
        weighted = column(colA, 0, i) * k[rows, :].astype(F32)
        normal = normal + jnp.sum(weighted, axis=0, keepdims=True)
        state = state + tn(weighted.astype(BF16), v[rows, :])
    ustate[...] = state
    lane128 = lax.broadcasted_iota(jnp.int32, (1, 128), 1)
    bsend[0:1, :] = normal[:, 0:128]
    bsend[1:2, :] = normal[:, 128:256]
    bsend[2:3, :] = jnp.where(lane128 < 64, keep_all + best_all, keep_all)
    placed = jnp.concatenate([inn[...], jnp.zeros((1, 120), F32)], axis=1)
    bsend[3:4, :] = pltpu.roll(placed, 8 * lax.rem(sp, 16), 1)

    phase("pack")
    def pack_slab(j, carry):
        slab = ustate[pl.ds(pl.multiple_of(8 * j, 8), 8), :]
        usend[j] = jnp.concatenate([slab[:, 0:128], slab[:, 128:256]], axis=0).astype(BF16)
        return carry

    lax.fori_loop(0, NSP, pack_slab, 0)
    urecv[sp] = usend[sp]
    brecv[sp] = bsend[...]

    phase("barrier")
    pl.semaphore_wait(barrier, NSP - 1 + NTP - 1)

    def b_copy(dst):
        return pltpu.make_async_remote_copy(
            src_ref=bsend, dst_ref=brecv.at[sp], send_sem=bsem.at[0], recv_sem=bsem.at[1 + sp // HALF],
            device_id={"sp": dst, "tp": tp}, device_id_type=MESH,
        )

    def u_copy(dst):
        return pltpu.make_async_remote_copy(
            src_ref=usend.at[dst], dst_ref=urecv.at[sp], send_sem=usem.at[0], recv_sem=usem.at[1 + sp // HALF],
            device_id={"sp": dst, "tp": tp}, device_id_type=MESH,
        )

    def s_copy(dst):
        return pltpu.make_async_remote_copy(
            src_ref=ssend.at[dst], dst_ref=srecv.at[sp], send_sem=ssem.at[0], recv_sem=ssem.at[1],
            device_id={"sp": dst, "tp": tp}, device_id_type=MESH,
        )

    def send_first(n, carry):
        dst = sp_peer(n)
        b_copy(dst).start()
        u_copy(dst).start()
        return carry

    def send_second(half):
        def send(n, carry):
            dst = HALF * half + lax.rem(sp + HALF // 2 + n, HALF)

            @pl.when(dst != sp)
            def _():
                s_copy(dst).start()

            return carry

        lax.fori_loop(0, HALF, send, 0)

    def wait_first(half):
        def wait(count):
            pltpu.make_async_copy(brecv.at[pl.ds(0, count)], brecv.at[pl.ds(0, count)], bsem.at[1 + half]).wait()
            pltpu.make_async_copy(urecv.at[pl.ds(0, count)], urecv.at[pl.ds(0, count)], usem.at[1 + half]).wait()

        @pl.when(sp // HALF == half)
        def _():
            wait(HALF - 1)

        @pl.when(sp // HALF != half)
        def _():
            wait(HALF)

    phase("send1")
    lax.fori_loop(0, NSP - 1, send_first, 0)
    w_copies = [
        pltpu.make_async_remote_copy(
            src_ref=src, dst_ref=dst, send_sem=wsend.at[i], recv_sem=wrecv.at[i], device_id=sib, device_id_type=MESH
        )
        for i, (src, dst) in enumerate([(w_out_memory, wom.at[pl.ds(H, H)]), (w_out_pool, wop.at[pl.ds(G, G)])])
    ]
    for copy in w_copies:
        copy.start()

    halo = pltpu.make_async_remote_copy(
        src_ref=pool_ext.at[pl.ds(T, HALO)], dst_ref=pool_ext.at[pl.ds(0, HALO)], send_sem=hsem.at[0],
        recv_sem=hsem.at[1], device_id={"sp": lax.rem(sp + 1, NSP), "tp": tp}, device_id_type=MESH,
    )

    @pl.when(sp < NSP - 1)
    def _():
        halo.start()

    phase("pgate")
    for i in range(11, 17):
        copies[i].wait()
    for i in range(2):
        rows = pl.ds(512 * i, 512)
        pgate[rows, :] = silu(nn(nrm[rows, :], wpg[...])) * pg[...]

    def p_copy(n):
        return pltpu.make_async_remote_copy(
            src_ref=pbuf.at[2 * n + 1 - c], dst_ref=psib.at[n], send_sem=psem.at[0], recv_sem=psem.at[1],
            device_id=sib, device_id_type=MESH,
        )

    order = (2, 1, 3, 0)

    def rs_copy(n, src, dst, to):
        return pltpu.make_async_remote_copy(
            src_ref=src, dst_ref=dst, send_sem=rsend.at[n], recv_sem=rrecv.at[n], device_id=to, device_id_type=MESH
        )

    rs = [
        rs_copy(0, part.at[2, 0], r1, up), rs_copy(1, part.at[2, 1], r2, down),
        rs_copy(2, part.at[1, 1], r3, up), rs_copy(3, part.at[3, 0], r4, down),
        rs_copy(4, fwd.at[0], r5, up), rs_copy(5, fwd.at[1], r6, down),
        rs_copy(6, ppart.at[0], rp1, up), rs_copy(7, ppart.at[1], rp2, down),
    ]

    def memory_inputs(dy):
        to = lax.rem(y + dy, NY)
        return jnp.concatenate([zbuf[2 * to + c], zsib[to]], axis=1)

    def pool_inputs(dy):
        to = lax.rem(y + dy, NY)
        return jnp.concatenate([pbuf[2 * to + c], psib[to]], axis=1)

    phase("q")
    for i in range(2):
        rows = pl.ds(512 * i, 512)
        q[rows, :] = nn(nrm[rows, :], wq[...]).astype(BF16)

    memory = jnp.concatenate([im[:, 0:128], im[:, 128:256]], axis=0)
    stab = jnp.zeros((1, 1), F32)
    my_stab = jnp.zeros((1, 1), F32)
    carried_n = jnp.zeros((2, 128), F32)
    my_n = carried_n
    fade_all = jnp.ones((1, 1), F32)
    my_fade = fade_all
    for half in range(2):
        phase("wait1_%d" % half)
        wait_first(half)
        phase("scan%d" % half)
        for j in range(HALF * half, HALF * half + HALF):
            mine = sp == j
            my_stab = jnp.where(mine, stab, my_stab)
            my_n = jnp.where(mine, carried_n, my_n)
            my_fade = jnp.where(mine, fade_all, my_fade)
            ssend[j] = memory.astype(BF16)
            piece_stab = brecv[j, 2:3, 0:1]
            piece_keep = brecv[j, 2:3, 64:65]
            new_stab = jnp.maximum(stab + piece_keep, piece_stab)
            fade = jnp.exp(stab + piece_keep - new_stab)
            weight = jnp.exp(piece_stab - new_stab)
            memory = fade * memory + weight * urecv[j].astype(F32)
            carried_n = fade * carried_n + weight * brecv[j, 0:2, :]
            fade_all = fade_all * fade
            stab = new_stab

        phase("send2_%d" % half)

        @pl.when(sp // HALF == half)
        def _():
            srecv[sp] = ssend[sp]

        send_second(half)
        if half == 0:
            phase("pool")
            @pl.when(sp > 0)
            def _():
                halo.wait_recv()

            @pl.when(sp == 0)
            def _():
                pool_ext[pl.ds(0, HALO), :] = jnp.zeros((HALO, G), BF16)

            window = lax.shift_left(jnp.int32(2), tp)
            for i in range(4):
                rows = pl.ds(256 * i, 256)
                near = pool_ext[pl.ds(256 * i, 512), :]
                target = lax.broadcasted_iota(jnp.int32, (256, 512), 0) + HALO
                back = target - lax.broadcasted_iota(jnp.int32, (256, 512), 1)
                band = jnp.where((back >= 0) & (back < window), 1.0, 0.0).astype(BF16)
                sums = nn(band, near)
                place = sp * T + 256 * i + lax.broadcasted_iota(jnp.int32, (256, 1), 0) + 1
                count = jnp.minimum(place, window).astype(F32)
                pooled = (sums / count - near[HALO:, :].astype(F32)).astype(BF16)
                mixed = nn(pooled, pm[...]) * pgate[rows, :]
                pbuf[2 * i] = mixed[0:128].astype(BF16)
                pbuf[2 * i + 1] = mixed[128:256].astype(BF16)

            for n in range(NY):
                p_copy(n).start()

            phase("attn")
            head_scale = H ** (-0.5)
            for i in range(4):
                rows = pl.ds(256 * i, 256)
                length = 256 * (i + 1)
                scores = nt(q[rows, :], k[pl.ds(0, length), :])
                source = jnp.concatenate([offer[r : r + 1, :] for r in range(2 * (i + 1))], axis=1)
                exponent = source - column(colA, 1, i)
                ahead = lax.broadcasted_iota(jnp.int32, (256, length), 1) > lax.broadcasted_iota(
                    jnp.int32, (256, length), 0
                ) + 256 * i
                weights = jnp.exp(jnp.where(ahead, NEG, exponent)) * scores * head_scale
                den[rows, :] = jnp.broadcast_to(jnp.sum(weights, axis=1, keepdims=True), (256, 128))
                num[rows, :] = nn(weights.astype(BF16), v[pl.ds(0, length), :])

    phase("pout")
    for i in range(17, 20):
        copies[i].wait()
    for copy in w_copies:
        copy.wait_recv()
    pltpu.make_async_copy(psib, psib, psem.at[1]).wait()
    pool_in = pool_inputs(2)
    for quarter in range(4):
        at = pl.ds(512 * (quarter % 2), 512)
        ppart[quarter // 2, :, at] = nn(pool_in, wop[:, pl.ds(512 * quarter, 512)]).astype(BF16)
    rs[6].start()
    rs[7].start()

    start_low = jnp.zeros((1, 128), F32)
    start_high = jnp.zeros((1, 128), F32)
    for j in range(HALF):
        start_low = start_low + brecv[j, 3:4, :]
        start_high = start_high + brecv[HALF + j, 3:4, :]
    my_n = my_n + my_fade * jnp.concatenate([start_low, start_high], axis=0)

    phase("gate")
    for i in range(2):
        rows = pl.ds(512 * i, 512)
        gate[rows, :] = silu(nn(nrm[rows, :], wg[...])) * mg[...]

    phase("denom")
    joint = jnp.maximum(best, my_stab)
    local_weight = jnp.exp(best - joint)
    carry_weight = jnp.exp(my_stab - joint) * head_scale
    least = jnp.exp(-(keep_run + joint))
    cols[...] = columns_of([local_weight, carry_weight, least])
    n_row = jnp.concatenate([my_n[0:1, :], my_n[1:2, :]], axis=1)
    colB = cols[...]
    for i in range(4):
        rows = pl.ds(256 * i, 256)
        carried = jnp.sum(q[rows, :].astype(F32) * n_row, axis=1, keepdims=True)
        full = den[rows, 0:1] * column(colB, 0, i) + column(colB, 1, i) * carried
        inverse = 1.0 / jnp.maximum(jnp.abs(full), column(colB, 2, i))
        num[rows, :] = num[rows, :] * (column(colB, 0, i) * inverse)
        den[rows, :] = jnp.broadcast_to(column(colB, 1, i) * inverse, (256, 128))

    phase("wait2")
    pltpu.make_async_copy(srecv.at[pl.ds(0, NSP - 1)], srecv.at[pl.ds(0, NSP - 1)], ssem.at[1]).wait()
    phase("finish")
    for j in range(NSP):
        slab = srecv[j].astype(F32)
        smat[8 * j : 8 * j + 8, 0:128] = slab[0:8]
        smat[8 * j : 8 * j + 8, 128:256] = slab[8:16]
    held = smat[...].astype(BF16)
    lane_sq = lax.broadcasted_iota(jnp.int32, (128, 128), 1)
    squares = jnp.zeros((128, 128), F32)

    def z_copy(n):
        to = lax.rem(y + order[n], NY)
        return pltpu.make_async_remote_copy(
            src_ref=zbuf.at[2 * to + 1 - c], dst_ref=zsib.at[to], send_sem=zsem.at[n], recv_sem=zsem.at[NY + n],
            device_id=sib, device_id_type=MESH,
        )

    z_copies = [z_copy(n) for n in range(NY)]
    for n in range(NY):
        for core in (1 - c, c):
            block = 2 * lax.rem(y + order[n], NY) + core
            rows = pl.ds(pl.multiple_of(128 * block, 128), 128)
            memory_rows = num[rows, :] + den[rows, 0:1] * nn(q[rows, :], held)
            sq = jnp.sum(memory_rows * memory_rows, axis=1, keepdims=True)
            squares = jnp.where(lane_sq == block, sq, squares)
            zbuf[block] = (memory_rows * gate[rows, :]).astype(BF16)
        z_copies[n].start()
    own_sq = squares.T[0:8]
    sqs[...] = own_sq

    def sq_copy(n):
        return pltpu.make_async_remote_copy(
            src_ref=sqs, dst_ref=sqr.at[n], send_sem=qsem.at[0], recv_sem=qsem.at[1],
            device_id={"sp": sp, "tp": lax.rem(tp + n + 1, NTP)}, device_id_type=MESH,
        )

    for n in range(NTP - 1):
        sq_copy(n).start()
    eye = lax.broadcasted_iota(jnp.int32, (128, 128), 0) == lax.broadcasted_iota(jnp.int32, (128, 128), 1)

    def out_scale(dy):
        to = lax.rem(y + dy, NY)
        row = cols[pl.ds(2 * to + c, 1), :]
        return jnp.sum(jnp.where(eye, jnp.broadcast_to(row, (128, 128)), 0.0), axis=1, keepdims=True)

    phase("zwait")
    z_copies[0].wait_recv()
    phase("ob2")
    memory_in = memory_inputs(2)
    for half in range(2):
        for quarter in range(2):
            at = pl.ds(512 * quarter, 512)
            part[2, half, :, at] = nn(memory_in, wom[:, pl.ds(1024 * half + 512 * quarter, 512)]).astype(BF16)
        rs[half].start()

    phase("sqwait")
    pltpu.make_async_copy(sqr, sqr, qsem.at[1]).wait()
    phase("scale")
    total = own_sq
    for n in range(NTP - 1):
        total = total + sqr[n]
    cols[0:8, :] = lax.rsqrt(total / (NTP * H) + EPS)
    for n, dy in ((1, 1), (2, 3), (3, 0)):
        phase("ob%d" % dy)
        z_copies[n].wait_recv()
        memory_in, pool_in = memory_inputs(dy), pool_inputs(dy)
        scale = out_scale(dy)
        for half in (1, 0) if dy == 1 else (0, 1):
            for quarter in range(2):
                at = pl.ds(1024 * half + 512 * quarter, 512)
                term = nn(memory_in, wom[:, at]) * scale + nn(pool_in, wop[:, at])
                part[dy, half, :, pl.ds(512 * quarter, 512)] = term.astype(BF16)
            if dy and half == dy % 3:
                rs[1 + dy - dy // 2].start()

    phase("drain")
    all_b = brecv.at[pl.ds(0, NSP - 1)]
    all_u = urecv.at[pl.ds(0, NSP - 1)]
    pltpu.make_async_copy(all_b, all_b, bsem.at[0]).wait()
    pltpu.make_async_copy(all_u, all_u, usem.at[0]).wait()
    pltpu.make_async_copy(all_u, all_u, ssem.at[0]).wait()
    for copy in w_copies + z_copies + [rs[6], rs[7]]:
        copy.wait_send()

    @pl.when(sp < NSP - 1)
    def _():
        halo.wait_send()

    pltpu.make_async_copy(psib, psib, psem.at[0]).wait()
    pltpu.make_async_copy(sqr, sqr, qsem.at[0]).wait()
    rs[6].wait_recv()
    rs[7].wait_recv()

    phase("rw0")
    rs[0].wait_recv()
    phase("fwd0")
    fwd[0] = (part[1, 0].astype(F32) + rp1[...].astype(F32) + out_scale(1) * r1[...].astype(F32)).astype(BF16)
    rs[4].start()
    phase("rw1")
    rs[1].wait_recv()
    phase("fwd1")
    fwd[1] = (part[3, 1].astype(F32) + rp2[...].astype(F32) + out_scale(3) * r2[...].astype(F32)).astype(BF16)
    rs[5].start()
    phase("rw2")
    for n in range(2, 4):
        rs[n].wait_recv()
    for n in range(4):
        rs[n].wait_send()
    phase("rw4")
    for n in range(4, 6):
        rs[n].wait_recv()
    phase("final")
    low = part[0, 0].astype(F32) + r4[...].astype(F32) + r5[...].astype(F32)
    high = part[0, 1].astype(F32) + r3[...].astype(F32) + r6[...].astype(F32)
    mean = (jnp.sum(low * low, axis=1, keepdims=True) + jnp.sum(high * high, axis=1, keepdims=True)) / D
    scale = lax.rsqrt(mean + EPS)
    out[:, 0:1024] = (low * scale * post[:, 0:1024]).astype(BF16)
    out[:, 1024:2048] = (high * scale * post[:, 1024:2048]).astype(BF16)
    for n in range(4, 6):
        rs[n].wait_send()
    phase(None)


def body(
    tokens, pre_gain, w_query, w_key, w_value, memory_output_gate_weight, w_input_gate, w_forget_gate, input_bias,
    forget_bias, forget_extra, initial_memory, initial_normal, memory_gain, w_pool_input, w_pool_gate, pool_mix,
    pool_gain, w_out_memory, w_out_pool, post_gain,
):
    args = (
        tokens, pre_gain.reshape(1, D), w_query, w_key, w_value, memory_output_gate_weight, w_input_gate.T,
        w_forget_gate.T, input_bias.reshape(1, 8), forget_bias.reshape(1, 8), forget_extra.reshape(8, 128),
        initial_memory.reshape(8, H), initial_normal, memory_gain.reshape(1, D), w_pool_input, w_pool_gate, pool_mix,
        pool_gain.reshape(1, NTP * G), w_out_memory, w_out_pool, post_gain.reshape(1, D),
    )
    vmem = pltpu.VMEM
    dma = pltpu.SemaphoreType.DMA
    scratch = [
        vmem((T, D), BF16), vmem((T, D), BF16), vmem((D, H), BF16), vmem((D, H), BF16), vmem((D, H), BF16),
        vmem((D, H), BF16), vmem((D, 2 * G), BF16), vmem((D, G), BF16), vmem((16, D), BF16), vmem((1, D), F32), vmem((1, 8), F32),
        vmem((1, 8), F32), vmem((8, 128), F32), vmem((8, H), F32), vmem((1, 8), F32), vmem((1, H), F32),
        vmem((G, G), BF16), vmem((1, G), F32), vmem((2 * H, D), BF16), vmem((2 * G, D), BF16), vmem((1, D), F32),
        vmem((T, 128), F32), vmem((T, H), BF16), vmem((T, H), BF16), vmem((T, H), BF16), vmem((T, H), F32),
        vmem((HALO + T, G), BF16), vmem((T, G), F32), vmem((T, H), F32), vmem((T, 128), F32), vmem((128, 128), F32),
        vmem((H, H), F32), vmem((NSP, 16, 128), BF16), vmem((NSP, 16, 128), BF16), vmem((4, 128), F32),
        vmem((NSP, 4, 128), F32), vmem((NSP, 16, 128), BF16), vmem((NSP, 16, 128), BF16), vmem((H, H), F32),
        vmem((8, 128), F32), vmem((NTP - 1, 8, 128), F32), vmem((NTP, 128, H), BF16), vmem((NY, 128, H), BF16),
        vmem((NTP, 128, G), BF16), vmem((NY, 128, G), BF16),
        vmem((2, 128, 1024), BF16), vmem((NY, 2, 128, 1024), BF16), vmem((2, 128, 1024), BF16), vmem((128, 1024), BF16), vmem((128, 1024), BF16),
        vmem((128, 1024), BF16), vmem((128, 1024), BF16), vmem((128, 1024), BF16), vmem((128, 1024), BF16),
        vmem((128, 1024), BF16), vmem((128, 1024), BF16),
        dma((20,)), dma((4,)), dma((2,)), dma((2,)), dma((3,)), dma((3,)), dma((2,)), dma((2,)), dma((2,)),
        dma((2 * NY,)), dma((2,)), dma((8,)), dma((8,)),
    ]
    anywhere = pl.BlockSpec(memory_space=pltpu.HBM)
    return pl.pallas_call(
        kernel,
        out_shape=jax.ShapeDtypeStruct((128, D), BF16),
        in_specs=[anywhere] * len(args),
        out_specs=pl.BlockSpec(memory_space=pltpu.VMEM),
        scratch_shapes=scratch,
        compiler_params=pltpu.CompilerParams(
            collective_id=0, has_side_effects=True, vmem_limit_bytes=48 * 1024 * 1024
        ),
    )(*[pltpu.with_memory_space_constraint(a, pltpu.HBM) for a in args])


def solution(mesh):
    in_specs = (
        P("sp", None), P(), P(None, "tp"), P(None, "tp"), P(None, "tp"), P(None, "tp"), P(), P(), P(), P(),
        P("sp", "tp"), P("tp", "sp", None), P("tp", "sp"), P(), P(None, "tp"), P(None, "tp"), P(), P(),
        P("tp", None), P("tp", None), P(),
    )
    return jax.shard_map(
        body, mesh=mesh, in_specs=in_specs, out_specs=P(("sp", "tp"), None), check_vma=False
    )
```

time: 59.8 us -> 50.5 us (0.84)
  Pallas kernels: 57.8 us -> 49.6 us
  local copies, waits for them, and re-layouts: 1.88 us -> 0.8 us
    pallas_call x1, Pallas kernels: 57.8 us -> 49.6 us  [body(): pl.pallas_call(kernel, out_shape=jax.ShapeDtypeStruct((128, D), BF16), in...]
    unnamed x1, local copies, waits for them, and re-layouts: 1.88 us -> 0.8 us
where the time goes in v2:
time: 50.5 us
  Pallas kernels  49.6 us (98%)
  local copies, waits for them, and re-layouts  0.8 us (2%)
    pallas_call x1, Pallas kernels, body(): pl.pallas_call(kernel, out_shape=jax.ShapeDtypeStruct((128, D), BF16), in...  49.6 us

profile of v2, /device:TPU:1, one launch (start us, length us, event | category | flops | bytes accessed | tf_op | source)
XLA Modules:
  0.0 50.5 jit_solution(8087937079893646594)
XLA Ops:
  0.0 49.6 %shard_map.199 = bf16[128,2048]{1,0:T(8,128)(2,1)S(1)} custom-call(bf16[1024,2048]{1,0:T(8,128)(2,1)} %tokens.1, f32[1,2048]{1,0:T(1,128)} %bitcast.12, bf16[2048,256]{1,0:T(8,128)(2,1)} %w_query.1, bf16[2048,256]{1,0:T(8,128)(2,1)} %w_key.1, bf16[2048,256]{1,0:T(8,128)(2,1)} %w_value.1, bf16[2048,256]{1,0:T(8,128)(2,1)} %w_gate.1, ...), custom_call_target="tpu_custom_call" | custom-call | tf_op jit(solution)/shard_map/pallas_call | solution.py:611
  49.7 0.8 %copy.23 = bf16[128,2048]{1,0:T(8,128)(2,1)} copy(bf16[128,2048]{1,0:T(8,128)(2,1)S(1)} %shard_map.199) | data formatting | bytes 1048576

commit v3 on v2

--- a/solution.py
+++ b/solution.py
@@ -20,6 +20,8 @@
 NTP = 8
 NY = 4
 HALF = NSP // 2
+STAGES = ((0, 8), (8, 8), (16, 16))
+CHUNKS = ((0, 256), (256, 256), (512, 256), (768, 256))
 HALO = 256
 
 
@@ -86,16 +88,14 @@
     down = {"sp": sp, "tp": 2 * lax.rem(y + NY - 1, NY) + c}
 
     def sp_peer(n):
-        kz = n // NX
-        dz = lax.rem(4 + (kz + 1) // 2 * (1 - 2 * lax.rem(kz, 2)) + NZ, NZ)
-        dx = lax.rem(2 + lax.rem(n, NX), NX)
-        dx = jnp.where(lax.rem(n, NX) == 1, 1, jnp.where(lax.rem(n, NX) == 2, 3, jnp.where(lax.rem(n, NX) == 3, 0, 2)))
+        dz, dx = (4, 5, 3, 6, 2, 7, 1, 0)[n // NX], (2, 1, 3, 0)[n % NX]
         return lax.rem(z + dz, NZ) * NX + lax.rem(x + dx, NX)
 
     phase = Phases()
     phase("loads")
     tok_copies = [
-        pltpu.make_async_copy(tokens.at[pl.ds(256 * i, 256)], tok.at[pl.ds(256 * i, 256)], tsem.at[i]) for i in range(4)
+        pltpu.make_async_copy(tokens.at[pl.ds(at, size)], tok.at[pl.ds(at, size)], tsem.at[i])
+        for i, (at, size) in enumerate(CHUNKS)
     ]
     loads = [
         (pre_gain, pre), (w_in, gw.at[pl.ds(0, 8)]), (w_forget, gw.at[pl.ds(8, 8)]), (w_key, wk),
@@ -108,32 +108,22 @@
     ]
     copies = [pltpu.make_async_copy(src, dst, lsem.at[i]) for i, (src, dst) in enumerate(loads)]
     tok_copies[0].start()
-    for copy in copies[0:3]:
+    for copy in (*copies[0:3], tok_copies[1], copies[3], copies[4], *tok_copies[2:]):
         copy.start()
-    tok_copies[1].start()
-    copies[3].start()
-    copies[4].start()
-    tok_copies[2].start()
-    tok_copies[3].start()
-
+
+    pool_ext[pl.ds(0, HALO), :] = jnp.zeros((HALO, G), BF16)
     phase("greet")
     barrier = pltpu.get_barrier_semaphore()
 
-    def greet_sp(n, carry):
+    for n in range(NSP - 1):
         pl.semaphore_signal(barrier, inc=1, device_id={"sp": sp_peer(n), "tp": tp}, device_id_type=MESH)
-        return carry
-
-    def greet_tp(n, carry):
+    for n in range(1, NTP):
         pl.semaphore_signal(barrier, inc=1, device_id={"sp": sp, "tp": lax.rem(tp + n, NTP)}, device_id_type=MESH)
-        return carry
-
-    lax.fori_loop(0, NSP - 1, greet_sp, 0)
-    lax.fori_loop(1, NTP, greet_tp, 0)
 
     def norm_rows(i):
         tok_copies[i].wait()
-        rows = pl.ds(256 * i, 256)
-        total = jnp.zeros((256, 128), F32)
+        rows = pl.ds(*CHUNKS[i])
+        total = jnp.zeros((CHUNKS[i][1], 128), F32)
         for col in range(D // 128):
             piece = tok[rows, pl.ds(128 * col, 128)].astype(F32)
             total = total + piece * piece
@@ -143,27 +133,28 @@
             piece = tok[rows, at].astype(F32)
             nrm[rows, at] = (piece * scale * pre[:, at]).astype(BF16)
 
+    phase("norm0")
+    copies[0].wait()
+    norm_rows(0)
+    for copy in copies[5:]:
+        copy.start()
+    for i in (4, 3):
+        copies[i].wait()
     phase("gw")
-    for i in (0, 1, 2):
+    for i in (1, 2):
         copies[i].wait()
     for col in range(D // 128):
         at = pl.ds(128 * col, 128)
         logits = jnp.concatenate([gw[:, at].astype(F32), jnp.zeros((112, 128), F32)], axis=0)
         wp[at, G : 2 * G] = logits.T.astype(BF16)
-    phase("norm0")
-    norm_rows(0)
-    for copy in copies[5:]:
-        copy.start()
-    for i in (3, 4):
-        copies[i].wait()
-    for i in range(4):
+    for i, (at, size) in enumerate(CHUNKS):
         phase("kv%d" % i)
         if i < 3:
             norm_rows(i + 1)
-        rows = pl.ds(256 * i, 256)
+        rows = pl.ds(at, size)
         normed = nrm[rows, :]
         both = nn(normed, wp[...])
-        pool_ext[pl.ds(HALO + 256 * i, 256), :] = both[:, 0:G].astype(BF16)
+        pool_ext[pl.ds(HALO + at, size), :] = both[:, 0:G].astype(BF16)
         gz[rows, :] = both[:, G : 2 * G]
         k[rows, :] = nn(normed, wk[...]).astype(BF16)
     phase("gates")
@@ -187,15 +178,35 @@
     log_keep = jnp.minimum(pre_keep, 0.0) - jnp.log1p(jnp.exp(-jnp.abs(pre_keep))) + fex[...]
     keep_run = scan_packed(log_keep, jnp.add, 0.0)
     offer = log_input - keep_run
-    best = scan_packed(offer, jnp.maximum, NEG)
     keep_all = keep_run[7:8, 127:128]
-    best_all = best[7:8, 127:128]
+    best_all = jnp.max(jnp.max(offer, axis=0, keepdims=True), axis=1, keepdims=True)
     write = jnp.exp(offer - best_all)
-    colA = columns_of([write, best])
+    colA = columns_of([write])
 
     def column(source, index, i):
         at = 8 * index + 2 * i
         return jnp.concatenate([source[:, at : at + 1], source[:, at + 1 : at + 2]], axis=0)
+
+    phase("barrier")
+    pl.semaphore_wait(barrier, NSP - 1 + NTP - 1)
+
+    def halo_copy(size):
+        return pltpu.make_async_remote_copy(
+            src_ref=pool_ext.at[pl.ds(HALO + T - size, size)], dst_ref=pool_ext.at[pl.ds(HALO - size, size)],
+            send_sem=hsem.at[0], recv_sem=hsem.at[1], device_id={"sp": lax.rem(sp + 1, NSP), "tp": tp},
+            device_id_type=MESH,
+        )
+
+    def with_halo(there, act):
+        @pl.when(there & (tp < 6))
+        def _():
+            act(halo_copy(64))
+
+        @pl.when(there & (tp >= 6))
+        def _():
+            act(halo_copy(HALO))
+
+    with_halo(sp < NSP - 1, lambda copy: copy.start())
 
     phase("state")
     state = jnp.zeros((H, H), F32)
@@ -223,18 +234,17 @@
     urecv[sp] = usend[sp]
     brecv[sp] = bsend[...]
 
-    phase("barrier")
-    pl.semaphore_wait(barrier, NSP - 1 + NTP - 1)
+    my_stage = jnp.where(sp < STAGES[1][0], 0, jnp.where(sp < STAGES[2][0], 1, 2))
 
     def b_copy(dst):
         return pltpu.make_async_remote_copy(
-            src_ref=bsend, dst_ref=brecv.at[sp], send_sem=bsem.at[0], recv_sem=bsem.at[1 + sp // HALF],
+            src_ref=bsend, dst_ref=brecv.at[sp], send_sem=bsem.at[0], recv_sem=bsem.at[1 + my_stage],
             device_id={"sp": dst, "tp": tp}, device_id_type=MESH,
         )
 
     def u_copy(dst):
         return pltpu.make_async_remote_copy(
-            src_ref=usend.at[dst], dst_ref=urecv.at[sp], send_sem=usem.at[0], recv_sem=usem.at[1 + sp // HALF],
+            src_ref=usend.at[dst], dst_ref=urecv.at[sp], send_sem=usem.at[0], recv_sem=usem.at[1 + my_stage],
             device_id={"sp": dst, "tp": tp}, device_id_type=MESH,
         )
 
@@ -244,39 +254,36 @@
             device_id={"sp": dst, "tp": tp}, device_id_type=MESH,
         )
 
-    def send_first(n, carry):
-        dst = sp_peer(n)
-        b_copy(dst).start()
-        u_copy(dst).start()
-        return carry
-
-    def send_second(half):
-        def send(n, carry):
-            dst = HALF * half + lax.rem(sp + HALF // 2 + n, HALF)
+    def send_first():
+        for n in range(NSP - 1):
+            dst = sp_peer(n)
+            b_copy(dst).start()
+            u_copy(dst).start()
+
+    def send_second(stage):
+        first, size = STAGES[stage]
+        for n in range(size):
+            dst = first + lax.rem(sp + size // 2 + n, size)
 
             @pl.when(dst != sp)
             def _():
                 s_copy(dst).start()
 
-            return carry
-
-        lax.fori_loop(0, HALF, send, 0)
-
-    def wait_first(half):
+    def wait_first(stage):
         def wait(count):
-            pltpu.make_async_copy(brecv.at[pl.ds(0, count)], brecv.at[pl.ds(0, count)], bsem.at[1 + half]).wait()
-            pltpu.make_async_copy(urecv.at[pl.ds(0, count)], urecv.at[pl.ds(0, count)], usem.at[1 + half]).wait()
-
-        @pl.when(sp // HALF == half)
+            pltpu.make_async_copy(brecv.at[pl.ds(0, count)], brecv.at[pl.ds(0, count)], bsem.at[1 + stage]).wait()
+            pltpu.make_async_copy(urecv.at[pl.ds(0, count)], urecv.at[pl.ds(0, count)], usem.at[1 + stage]).wait()
+
+        @pl.when(my_stage == stage)
         def _():
-            wait(HALF - 1)
-
-        @pl.when(sp // HALF != half)
+            wait(STAGES[stage][1] - 1)
+
+        @pl.when(my_stage != stage)
         def _():
-            wait(HALF)
+            wait(STAGES[stage][1])
 
     phase("send1")
-    lax.fori_loop(0, NSP - 1, send_first, 0)
+    send_first()
     w_copies = [
         pltpu.make_async_remote_copy(
             src_ref=src, dst_ref=dst, send_sem=wsend.at[i], recv_sem=wrecv.at[i], device_id=sib, device_id_type=MESH
@@ -285,15 +292,6 @@
     ]
     for copy in w_copies:
         copy.start()
-
-    halo = pltpu.make_async_remote_copy(
-        src_ref=pool_ext.at[pl.ds(T, HALO)], dst_ref=pool_ext.at[pl.ds(0, HALO)], send_sem=hsem.at[0],
-        recv_sem=hsem.at[1], device_id={"sp": lax.rem(sp + 1, NSP), "tp": tp}, device_id_type=MESH,
-    )
-
-    @pl.when(sp < NSP - 1)
-    def _():
-        halo.start()
 
     phase("pgate")
     for i in range(11, 17):
@@ -334,6 +332,11 @@
     for i in range(2):
         rows = pl.ds(512 * i, 512)
         q[rows, :] = nn(nrm[rows, :], wq[...]).astype(BF16)
+
+    phase("gate")
+    for i in range(2):
+        rows = pl.ds(512 * i, 512)
+        gate[rows, :] = silu(nn(nrm[rows, :], wg[...])) * mg[...]
 
     memory = jnp.concatenate([im[:, 0:128], im[:, 128:256]], axis=0)
     stab = jnp.zeros((1, 1), F32)
@@ -342,11 +345,51 @@
     my_n = carried_n
     fade_all = jnp.ones((1, 1), F32)
     my_fade = fade_all
-    for half in range(2):
-        phase("wait1_%d" % half)
-        wait_first(half)
-        phase("scan%d" % half)
-        for j in range(HALF * half, HALF * half + HALF):
+    best = scan_packed(offer, jnp.maximum, NEG)
+    head_scale = H ** (-0.5)
+
+    def beside():
+        phase("pool")
+        with_halo(sp > 0, lambda copy: copy.wait_recv())
+        window = lax.shift_left(jnp.int32(2), tp)
+        for i in range(4):
+            rows = pl.ds(256 * i, 256)
+            near = pool_ext[pl.ds(256 * i, 512), :]
+            target = lax.broadcasted_iota(jnp.int32, (256, 512), 0) + HALO
+            back = target - lax.broadcasted_iota(jnp.int32, (256, 512), 1)
+            band = jnp.where((back >= 0) & (back < window), 1.0, 0.0).astype(BF16)
+            sums = nn(band, near)
+            place = sp * T + 256 * i + lax.broadcasted_iota(jnp.int32, (256, 1), 0) + 1
+            count = jnp.minimum(place, window).astype(F32)
+            pooled = (sums / count - near[HALO:, :].astype(F32)).astype(BF16)
+            mixed = nn(pooled, pm[...]) * pgate[rows, :]
+            pbuf[2 * i] = mixed[0:128].astype(BF16)
+            pbuf[2 * i + 1] = mixed[128:256].astype(BF16)
+
+        for n in range(NY):
+            p_copy(n).start()
+
+        phase("attn")
+        colC = columns_of([best])
+        for i in range(4):
+            rows = pl.ds(256 * i, 256)
+            length = 256 * (i + 1)
+            scores = nt(q[rows, :], k[pl.ds(0, length), :])
+            source = jnp.concatenate([offer[r : r + 1, :] for r in range(2 * (i + 1))], axis=1)
+            exponent = source - column(colC, 0, i)
+            ahead = lax.broadcasted_iota(jnp.int32, (256, length), 1) > lax.broadcasted_iota(
+                jnp.int32, (256, length), 0
+            ) + 256 * i
+            weights = jnp.exp(jnp.where(ahead, NEG, exponent)) * scores * head_scale
+            den[rows, :] = jnp.broadcast_to(jnp.sum(weights, axis=1, keepdims=True), (256, 128))
+            num[rows, :] = nn(weights.astype(BF16), v[pl.ds(0, length), :])
+
+
+    for stage, (first, size) in enumerate(STAGES):
+        phase("wait1_%d" % stage)
+        wait_first(stage)
+        phase("scan%d" % stage)
+        for j in range(first, first + size):
             mine = sp == j
             my_stab = jnp.where(mine, stab, my_stab)
             my_n = jnp.where(mine, carried_n, my_n)
@@ -362,55 +405,16 @@
             fade_all = fade_all * fade
             stab = new_stab
 
-        phase("send2_%d" % half)
-
-        @pl.when(sp // HALF == half)
+        phase("send2_%d" % stage)
+
+        @pl.when(my_stage == stage)
         def _():
             srecv[sp] = ssend[sp]
 
-        send_second(half)
-        if half == 0:
-            phase("pool")
-            @pl.when(sp > 0)
-            def _():
-                halo.wait_recv()
-
-            @pl.when(sp == 0)
-            def _():
-                pool_ext[pl.ds(0, HALO), :] = jnp.zeros((HALO, G), BF16)
-
-            window = lax.shift_left(jnp.int32(2), tp)
-            for i in range(4):
-                rows = pl.ds(256 * i, 256)
-                near = pool_ext[pl.ds(256 * i, 512), :]
-                target = lax.broadcasted_iota(jnp.int32, (256, 512), 0) + HALO
-                back = target - lax.broadcasted_iota(jnp.int32, (256, 512), 1)
-                band = jnp.where((back >= 0) & (back < window), 1.0, 0.0).astype(BF16)
-                sums = nn(band, near)
-                place = sp * T + 256 * i + lax.broadcasted_iota(jnp.int32, (256, 1), 0) + 1
-                count = jnp.minimum(place, window).astype(F32)
-                pooled = (sums / count - near[HALO:, :].astype(F32)).astype(BF16)
-                mixed = nn(pooled, pm[...]) * pgate[rows, :]
-                pbuf[2 * i] = mixed[0:128].astype(BF16)
-                pbuf[2 * i + 1] = mixed[128:256].astype(BF16)
-
-            for n in range(NY):
-                p_copy(n).start()
-
-            phase("attn")
-            head_scale = H ** (-0.5)
-            for i in range(4):
-                rows = pl.ds(256 * i, 256)
-                length = 256 * (i + 1)
-                scores = nt(q[rows, :], k[pl.ds(0, length), :])
-                source = jnp.concatenate([offer[r : r + 1, :] for r in range(2 * (i + 1))], axis=1)
-                exponent = source - column(colA, 1, i)
-                ahead = lax.broadcasted_iota(jnp.int32, (256, length), 1) > lax.broadcasted_iota(
-                    jnp.int32, (256, length), 0
-                ) + 256 * i
-                weights = jnp.exp(jnp.where(ahead, NEG, exponent)) * scores * head_scale
-                den[rows, :] = jnp.broadcast_to(jnp.sum(weights, axis=1, keepdims=True), (256, 128))
-                num[rows, :] = nn(weights.astype(BF16), v[pl.ds(0, length), :])
+        send_second(stage)
+        if stage == 1:
+            pl.when(sp < HALF)(beside)
+    pl.when(sp >= HALF)(beside)
 
     phase("pout")
     for i in range(17, 20):
@@ -431,11 +435,6 @@
         start_low = start_low + brecv[j, 3:4, :]
         start_high = start_high + brecv[HALF + j, 3:4, :]
     my_n = my_n + my_fade * jnp.concatenate([start_low, start_high], axis=0)
-
-    phase("gate")
-    for i in range(2):
-        rows = pl.ds(512 * i, 512)
-        gate[rows, :] = silu(nn(nrm[rows, :], wg[...])) * mg[...]
 
     phase("denom")
     joint = jnp.maximum(best, my_stab)
@@ -538,10 +537,7 @@
     for copy in w_copies + z_copies + [rs[6], rs[7]]:
         copy.wait_send()
 
-    @pl.when(sp < NSP - 1)
-    def _():
-        halo.wait_send()
-
+    with_halo(sp < NSP - 1, lambda copy: copy.wait_send())
     pltpu.make_async_copy(psib, psib, psem.at[0]).wait()
     pltpu.make_async_copy(sqr, sqr, qsem.at[0]).wait()
     rs[6].wait_recv()
@@ -604,7 +600,7 @@
         vmem((2, 128, 1024), BF16), vmem((NY, 2, 128, 1024), BF16), vmem((2, 128, 1024), BF16), vmem((128, 1024), BF16), vmem((128, 1024), BF16),
         vmem((128, 1024), BF16), vmem((128, 1024), BF16), vmem((128, 1024), BF16), vmem((128, 1024), BF16),
         vmem((128, 1024), BF16), vmem((128, 1024), BF16),
-        dma((20,)), dma((4,)), dma((2,)), dma((2,)), dma((3,)), dma((3,)), dma((2,)), dma((2,)), dma((2,)),
+        dma((20,)), dma((4,)), dma((2,)), dma((2,)), dma((4,)), dma((4,)), dma((2,)), dma((2,)), dma((2,)),
         dma((2 * NY,)), dma((2,)), dma((8,)), dma((8,)),
     ]
     anywhere = pl.BlockSpec(memory_space=pltpu.HBM)

time: 50.5 us -> 49.7 us (0.984)
  Pallas kernels: 49.6 us -> 48.8 us
    pallas_call x1, Pallas kernels: 49.6 us -> 48.8 us  [body(): pl.pallas_call(kernel, out_shape=jax.ShapeDtypeStruct((128, D), BF16), in...]
where the time goes in v3:
time: 49.7 us; the launch traced here: 49.6 us
  Pallas kernels  48.8 us (98%)
  local copies, waits for them, and re-layouts  0.8 us (2%)
    pallas_call x1, Pallas kernels, body(): pl.pallas_call(kernel, out_shape=jax.ShapeDtypeStruct((128, D), BF16), in...  48.8 us

profile of v3, /device:TPU:1, one launch (start us, length us, event | category | flops | bytes accessed | tf_op | source)
XLA Modules:
  0.0 49.6 jit_solution(5063742140748149234)
XLA Ops:
  0.0 48.8 %shard_map.199 = bf16[128,2048]{1,0:T(8,128)(2,1)S(1)} custom-call(bf16[1024,2048]{1,0:T(8,128)(2,1)} %tokens.1, f32[1,2048]{1,0:T(1,128)} %bitcast.12, bf16[2048,256]{1,0:T(8,128)(2,1)} %w_query.1, bf16[2048,256]{1,0:T(8,128)(2,1)} %w_key.1, bf16[2048,256]{1,0:T(8,128)(2,1)} %w_value.1, bf16[2048,256]{1,0:T(8,128)(2,1)} %w_gate.1, ...), custom_call_target="tpu_custom_call" | custom-call | tf_op jit(solution)/shard_map/pallas_call | solution.py:607
  48.8 0.8 %copy.23 = bf16[128,2048]{1,0:T(8,128)(2,1)} copy(bf16[128,2048]{1,0:T(8,128)(2,1)S(1)} %shard_map.199) | data formatting | bytes 1048576

commit v4 on v3

--- a/solution.py
+++ b/solution.py
@@ -75,9 +75,9 @@
     out,
     tok, nrm, wq, wk, wv, wg, wp, wpg, gw, pre, bias_i, bias_f, fex, im, inn, mg, pm, pg, wom, wop, post,
     gz, q, k, v, gate, pool_ext, pgate, num, den, cols,
-    ustate, usend, urecv, bsend, brecv, ssend, srecv, smat,
+    ustate, usend, urecv, arow, arecv, nrow, nrecv, ssend, srecv, smat,
     sqs, sqr, zbuf, zsib, pbuf, psib, ppart, part, fwd, r1, r2, r3, r4, r5, r6, rp1, rp2,
-    lsem, tsem, wsend, wrecv, usem, bsem, hsem, ssem, qsem, zsem, psem, rsend, rrecv,
+    lsem, tsem, wsend, wrecv, usem, bsem, nsem, hsem, ssem, qsem, zsem, psem, rsend, rrecv,
 ):
     sp = lax.axis_index("sp")
     tp = lax.axis_index("tp")
@@ -95,7 +95,7 @@
     phase("loads")
     tok_copies = [
         pltpu.make_async_copy(tokens.at[pl.ds(at, size)], tok.at[pl.ds(at, size)], tsem.at[i])
-        for i, (at, size) in enumerate(CHUNKS)
+        for i, (at, size) in enumerate(((0, 128), (128, 128), *CHUNKS[1:]))
     ]
     loads = [
         (pre_gain, pre), (w_in, gw.at[pl.ds(0, 8)]), (w_forget, gw.at[pl.ds(8, 8)]), (w_key, wk),
@@ -108,7 +108,7 @@
     ]
     copies = [pltpu.make_async_copy(src, dst, lsem.at[i]) for i, (src, dst) in enumerate(loads)]
     tok_copies[0].start()
-    for copy in (*copies[0:3], tok_copies[1], copies[3], copies[4], *tok_copies[2:]):
+    for copy in (copies[0], tok_copies[1], *copies[1:3], tok_copies[2], copies[3], copies[4], *tok_copies[3:]):
         copy.start()
 
     pool_ext[pl.ds(0, HALO), :] = jnp.zeros((HALO, G), BF16)
@@ -121,7 +121,8 @@
         pl.semaphore_signal(barrier, inc=1, device_id={"sp": sp, "tp": lax.rem(tp + n, NTP)}, device_id_type=MESH)
 
     def norm_rows(i):
-        tok_copies[i].wait()
+        for n in (0, 1) if i == 0 else (i + 1,):
+            tok_copies[n].wait()
         rows = pl.ds(*CHUNKS[i])
         total = jnp.zeros((CHUNKS[i][1], 128), F32)
         for col in range(D // 128):
@@ -218,11 +219,10 @@
         state = state + tn(weighted.astype(BF16), v[rows, :])
     ustate[...] = state
     lane128 = lax.broadcasted_iota(jnp.int32, (1, 128), 1)
-    bsend[0:1, :] = normal[:, 0:128]
-    bsend[1:2, :] = normal[:, 128:256]
-    bsend[2:3, :] = jnp.where(lane128 < 64, keep_all + best_all, keep_all)
-    placed = jnp.concatenate([inn[...], jnp.zeros((1, 120), F32)], axis=1)
-    bsend[3:4, :] = pltpu.roll(placed, 8 * lax.rem(sp, 16), 1)
+    nrow[0:1, :] = normal[:, 0:128]
+    nrow[1:2, :] = normal[:, 128:256]
+    placed = pltpu.roll(jnp.concatenate([inn[...], jnp.zeros((1, 120), F32)], axis=1), 64 + 8 * lax.rem(sp, 8), 1)
+    arow[...] = jnp.where(lane128 < 32, keep_all + best_all, jnp.where(lane128 < 64, keep_all, placed))
 
     phase("pack")
     def pack_slab(j, carry):
@@ -232,13 +232,20 @@
 
     lax.fori_loop(0, NSP, pack_slab, 0)
     urecv[sp] = usend[sp]
-    brecv[sp] = bsend[...]
+    arecv[sp] = arow[...]
+    nrecv[sp] = nrow[...]
 
     my_stage = jnp.where(sp < STAGES[1][0], 0, jnp.where(sp < STAGES[2][0], 1, 2))
 
     def b_copy(dst):
         return pltpu.make_async_remote_copy(
-            src_ref=bsend, dst_ref=brecv.at[sp], send_sem=bsem.at[0], recv_sem=bsem.at[1 + my_stage],
+            src_ref=arow, dst_ref=arecv.at[sp], send_sem=bsem.at[0], recv_sem=bsem.at[1 + my_stage],
+            device_id={"sp": dst, "tp": tp}, device_id_type=MESH,
+        )
+
+    def n_copy(dst):
+        return pltpu.make_async_remote_copy(
+            src_ref=nrow, dst_ref=nrecv.at[sp], send_sem=nsem.at[0], recv_sem=nsem.at[1],
             device_id={"sp": dst, "tp": tp}, device_id_type=MESH,
         )
 
@@ -259,6 +266,8 @@
             dst = sp_peer(n)
             b_copy(dst).start()
             u_copy(dst).start()
+        for n in range(NSP - 1):
+            n_copy(sp_peer(n)).start()
 
     def send_second(stage):
         first, size = STAGES[stage]
@@ -271,7 +280,7 @@
 
     def wait_first(stage):
         def wait(count):
-            pltpu.make_async_copy(brecv.at[pl.ds(0, count)], brecv.at[pl.ds(0, count)], bsem.at[1 + stage]).wait()
+            pltpu.make_async_copy(arecv.at[pl.ds(0, count)], arecv.at[pl.ds(0, count)], bsem.at[1 + stage]).wait()
             pltpu.make_async_copy(urecv.at[pl.ds(0, count)], urecv.at[pl.ds(0, count)], usem.at[1 + stage]).wait()
 
         @pl.when(my_stage == stage)
@@ -310,7 +319,7 @@
 
     def rs_copy(n, src, dst, to):
         return pltpu.make_async_remote_copy(
-            src_ref=src, dst_ref=dst, send_sem=rsend.at[n], recv_sem=rrecv.at[n], device_id=to, device_id_type=MESH
+            src_ref=src, dst_ref=dst, send_sem=rsend.at[0], recv_sem=rrecv.at[n], device_id=to, device_id_type=MESH
         )
 
     rs = [
@@ -341,10 +350,7 @@
     memory = jnp.concatenate([im[:, 0:128], im[:, 128:256]], axis=0)
     stab = jnp.zeros((1, 1), F32)
     my_stab = jnp.zeros((1, 1), F32)
-    carried_n = jnp.zeros((2, 128), F32)
-    my_n = carried_n
-    fade_all = jnp.ones((1, 1), F32)
-    my_fade = fade_all
+    steps = []
     best = scan_packed(offer, jnp.maximum, NEG)
     head_scale = H ** (-0.5)
 
@@ -384,7 +390,6 @@
             den[rows, :] = jnp.broadcast_to(jnp.sum(weights, axis=1, keepdims=True), (256, 128))
             num[rows, :] = nn(weights.astype(BF16), v[pl.ds(0, length), :])
 
-
     for stage, (first, size) in enumerate(STAGES):
         phase("wait1_%d" % stage)
         wait_first(stage)
@@ -392,17 +397,14 @@
         for j in range(first, first + size):
             mine = sp == j
             my_stab = jnp.where(mine, stab, my_stab)
-            my_n = jnp.where(mine, carried_n, my_n)
-            my_fade = jnp.where(mine, fade_all, my_fade)
             ssend[j] = memory.astype(BF16)
-            piece_stab = brecv[j, 2:3, 0:1]
-            piece_keep = brecv[j, 2:3, 64:65]
+            piece_stab = arecv[j, :, 0:1]
+            piece_keep = arecv[j, :, 32:33]
             new_stab = jnp.maximum(stab + piece_keep, piece_stab)
             fade = jnp.exp(stab + piece_keep - new_stab)
             weight = jnp.exp(piece_stab - new_stab)
             memory = fade * memory + weight * urecv[j].astype(F32)
-            carried_n = fade * carried_n + weight * brecv[j, 0:2, :]
-            fade_all = fade_all * fade
+            steps.append((fade, weight))
             stab = new_stab
 
         phase("send2_%d" % stage)
@@ -429,24 +431,33 @@
     rs[6].start()
     rs[7].start()
 
-    start_low = jnp.zeros((1, 128), F32)
-    start_high = jnp.zeros((1, 128), F32)
-    for j in range(HALF):
-        start_low = start_low + brecv[j, 3:4, :]
-        start_high = start_high + brecv[HALF + j, 3:4, :]
-    my_n = my_n + my_fade * jnp.concatenate([start_low, start_high], axis=0)
-
     phase("denom")
+    pltpu.make_async_copy(nrecv.at[pl.ds(0, NSP - 1)], nrecv.at[pl.ds(0, NSP - 1)], nsem.at[1]).wait()
+    quarters = []
+    for first in range(0, NSP, 8):
+        total = arecv[first]
+        for j in range(first + 1, first + 8):
+            total = total + arecv[j]
+        quarters.append(total)
+    my_n = jnp.concatenate(
+        [jnp.where(lane128 < 64, pltpu.roll(quarters[n], 64, 1), quarters[n + 1]) for n in (0, 2)], axis=0
+    )
+    for j, (fade, weight) in enumerate(steps[: NSP - 1]):
+        my_n = jnp.where(sp > j, fade * my_n + weight * nrecv[j], my_n)
     joint = jnp.maximum(best, my_stab)
     local_weight = jnp.exp(best - joint)
     carry_weight = jnp.exp(my_stab - joint) * head_scale
     least = jnp.exp(-(keep_run + joint))
     cols[...] = columns_of([local_weight, carry_weight, least])
     n_row = jnp.concatenate([my_n[0:1, :], my_n[1:2, :]], axis=1)
+    n_top = n_row.astype(BF16)
+    n_mid = (n_row - n_top.astype(F32)).astype(BF16)
+    n_low = (n_row - n_top.astype(F32) - n_mid.astype(F32)).astype(BF16)
+    n_rows = jnp.concatenate([n_top, n_mid, n_low, jnp.zeros((13, H), BF16)], axis=0)
     colB = cols[...]
     for i in range(4):
         rows = pl.ds(256 * i, 256)
-        carried = jnp.sum(q[rows, :].astype(F32) * n_row, axis=1, keepdims=True)
+        carried = jnp.sum(nt(q[rows, :], n_rows), axis=1, keepdims=True)
         full = den[rows, 0:1] * column(colB, 0, i) + column(colB, 1, i) * carried
         inverse = 1.0 / jnp.maximum(jnp.abs(full), column(colB, 2, i))
         num[rows, :] = num[rows, :] * (column(colB, 0, i) * inverse)
@@ -466,7 +477,7 @@
     def z_copy(n):
         to = lax.rem(y + order[n], NY)
         return pltpu.make_async_remote_copy(
-            src_ref=zbuf.at[2 * to + 1 - c], dst_ref=zsib.at[to], send_sem=zsem.at[n], recv_sem=zsem.at[NY + n],
+            src_ref=zbuf.at[2 * to + 1 - c], dst_ref=zsib.at[to], send_sem=zsem.at[NY], recv_sem=zsem.at[n],
             device_id=sib, device_id_type=MESH,
         )
 
@@ -529,13 +540,15 @@
                 rs[1 + dy - dy // 2].start()
 
     phase("drain")
-    all_b = brecv.at[pl.ds(0, NSP - 1)]
+    all_b = arecv.at[pl.ds(0, NSP - 1)]
+    pltpu.make_async_copy(nrecv.at[pl.ds(0, NSP - 1)], nrecv.at[pl.ds(0, NSP - 1)], nsem.at[0]).wait()
     all_u = urecv.at[pl.ds(0, NSP - 1)]
     pltpu.make_async_copy(all_b, all_b, bsem.at[0]).wait()
     pltpu.make_async_copy(all_u, all_u, usem.at[0]).wait()
     pltpu.make_async_copy(all_u, all_u, ssem.at[0]).wait()
-    for copy in w_copies + z_copies + [rs[6], rs[7]]:
+    for copy in w_copies:
         copy.wait_send()
+    pltpu.make_async_copy(zsib, zsib, zsem.at[NY]).wait()
 
     with_halo(sp < NSP - 1, lambda copy: copy.wait_send())
     pltpu.make_async_copy(psib, psib, psem.at[0]).wait()
@@ -556,20 +569,19 @@
     phase("rw2")
     for n in range(2, 4):
         rs[n].wait_recv()
-    for n in range(4):
-        rs[n].wait_send()
+    low = part[0, 0].astype(F32) + r4[...].astype(F32)
+    high = part[0, 1].astype(F32) + r3[...].astype(F32)
     phase("rw4")
     for n in range(4, 6):
         rs[n].wait_recv()
     phase("final")
-    low = part[0, 0].astype(F32) + r4[...].astype(F32) + r5[...].astype(F32)
-    high = part[0, 1].astype(F32) + r3[...].astype(F32) + r6[...].astype(F32)
+    low = low + r5[...].astype(F32)
+    high = high + r6[...].astype(F32)
     mean = (jnp.sum(low * low, axis=1, keepdims=True) + jnp.sum(high * high, axis=1, keepdims=True)) / D
     scale = lax.rsqrt(mean + EPS)
     out[:, 0:1024] = (low * scale * post[:, 0:1024]).astype(BF16)
     out[:, 1024:2048] = (high * scale * post[:, 1024:2048]).astype(BF16)
-    for n in range(4, 6):
-        rs[n].wait_send()
+    pltpu.make_async_copy(part, part, rsend.at[0]).wait()
     phase(None)
 
 
@@ -593,15 +605,15 @@
         vmem((G, G), BF16), vmem((1, G), F32), vmem((2 * H, D), BF16), vmem((2 * G, D), BF16), vmem((1, D), F32),
         vmem((T, 128), F32), vmem((T, H), BF16), vmem((T, H), BF16), vmem((T, H), BF16), vmem((T, H), F32),
         vmem((HALO + T, G), BF16), vmem((T, G), F32), vmem((T, H), F32), vmem((T, 128), F32), vmem((128, 128), F32),
-        vmem((H, H), F32), vmem((NSP, 16, 128), BF16), vmem((NSP, 16, 128), BF16), vmem((4, 128), F32),
-        vmem((NSP, 4, 128), F32), vmem((NSP, 16, 128), BF16), vmem((NSP, 16, 128), BF16), vmem((H, H), F32),
+        vmem((H, H), F32), vmem((NSP, 16, 128), BF16), vmem((NSP, 16, 128), BF16), vmem((1, 128), F32),
+        vmem((NSP, 1, 128), F32), vmem((2, 128), F32), vmem((NSP, 2, 128), F32), vmem((NSP, 16, 128), BF16), vmem((NSP, 16, 128), BF16), vmem((H, H), F32),
         vmem((8, 128), F32), vmem((NTP - 1, 8, 128), F32), vmem((NTP, 128, H), BF16), vmem((NY, 128, H), BF16),
         vmem((NTP, 128, G), BF16), vmem((NY, 128, G), BF16),
         vmem((2, 128, 1024), BF16), vmem((NY, 2, 128, 1024), BF16), vmem((2, 128, 1024), BF16), vmem((128, 1024), BF16), vmem((128, 1024), BF16),
         vmem((128, 1024), BF16), vmem((128, 1024), BF16), vmem((128, 1024), BF16), vmem((128, 1024), BF16),
         vmem((128, 1024), BF16), vmem((128, 1024), BF16),
-        dma((20,)), dma((4,)), dma((2,)), dma((2,)), dma((4,)), dma((4,)), dma((2,)), dma((2,)), dma((2,)),
-        dma((2 * NY,)), dma((2,)), dma((8,)), dma((8,)),
+        dma((20,)), dma((5,)), dma((2,)), dma((2,)), dma((4,)), dma((4,)), dma((2,)), dma((2,)), dma((2,)), dma((2,)),
+        dma((NY + 1,)), dma((2,)), dma((1,)), dma((8,)),
     ]
     anywhere = pl.BlockSpec(memory_space=pltpu.HBM)
     return pl.pallas_call(

time: 49.7 us -> 49.6 us (level)
  no operation moved by 1% of the time
where the time goes in v4:
time: 49.6 us
  Pallas kernels  48.8 us (98%)
  local copies, waits for them, and re-layouts  0.8 us (2%)
    pallas_call x1, Pallas kernels, body(): pl.pallas_call(kernel, out_shape=jax.ShapeDtypeStruct((128, D), BF16), in...  48.8 us

profile of v4, /device:TPU:1, one launch (start us, length us, event | category | flops | bytes accessed | tf_op | source)
XLA Modules:
  0.0 49.6 jit_solution(972286419660085188)
XLA Ops:
  0.0 48.8 %shard_map.199 = bf16[128,2048]{1,0:T(8,128)(2,1)S(1)} custom-call(bf16[1024,2048]{1,0:T(8,128)(2,1)} %tokens.1, f32[1,2048]{1,0:T(1,128)} %bitcast.12, bf16[2048,256]{1,0:T(8,128)(2,1)} %w_query.1, bf16[2048,256]{1,0:T(8,128)(2,1)} %w_key.1, bf16[2048,256]{1,0:T(8,128)(2,1)} %w_value.1, bf16[2048,256]{1,0:T(8,128)(2,1)} %w_gate.1, ...), custom_call_target="tpu_custom_call" | custom-call | tf_op jit(solution)/shard_map/pallas_call | solution.py:619
  48.8 0.8 %copy.23 = bf16[128,2048]{1,0:T(8,128)(2,1)} copy(bf16[128,2048]{1,0:T(8,128)(2,1)S(1)} %shard_map.199) | data formatting | bytes 1048576

commit v5 on v4

--- a/solution.py
+++ b/solution.py
@@ -342,11 +342,6 @@
         rows = pl.ds(512 * i, 512)
         q[rows, :] = nn(nrm[rows, :], wq[...]).astype(BF16)
 
-    phase("gate")
-    for i in range(2):
-        rows = pl.ds(512 * i, 512)
-        gate[rows, :] = silu(nn(nrm[rows, :], wg[...])) * mg[...]
-
     memory = jnp.concatenate([im[:, 0:128], im[:, 128:256]], axis=0)
     stab = jnp.zeros((1, 1), F32)
     my_stab = jnp.zeros((1, 1), F32)
@@ -414,6 +409,11 @@
             srecv[sp] = ssend[sp]
 
         send_second(stage)
+        if stage == 0:
+            phase("gate")
+            for i in range(2):
+                rows = pl.ds(512 * i, 512)
+                gate[rows, :] = silu(nn(nrm[rows, :], wg[...])) * mg[...]
         if stage == 1:
             pl.when(sp < HALF)(beside)
     pl.when(sp >= HALF)(beside)

time: 49.6 us -> 49.8 us (level)
  no operation moved by 1% of the time
where the time goes in v5:
time: 49.8 us; the launch traced here: 49.7 us
  Pallas kernels  48.9 us (98%)
  local copies, waits for them, and re-layouts  0.8 us (2%)
    pallas_call x1, Pallas kernels, body(): pl.pallas_call(kernel, out_shape=jax.ShapeDtypeStruct((128, D), BF16), in...  48.9 us

profile of v5, /device:TPU:1, one launch (start us, length us, event | category | flops | bytes accessed | tf_op | source)
XLA Modules:
  0.0 49.7 jit_solution(12595945295620098466)
XLA Ops:
  0.0 48.9 %shard_map.199 = bf16[128,2048]{1,0:T(8,128)(2,1)S(1)} custom-call(bf16[1024,2048]{1,0:T(8,128)(2,1)} %tokens.1, f32[1,2048]{1,0:T(1,128)} %bitcast.12, bf16[2048,256]{1,0:T(8,128)(2,1)} %w_query.1, bf16[2048,256]{1,0:T(8,128)(2,1)} %w_key.1, bf16[2048,256]{1,0:T(8,128)(2,1)} %w_value.1, bf16[2048,256]{1,0:T(8,128)(2,1)} %w_gate.1, ...), custom_call_target="tpu_custom_call" | custom-call | tf_op jit(solution)/shard_map/pallas_call | solution.py:619
  49.0 0.8 %copy.23 = bf16[128,2048]{1,0:T(8,128)(2,1)} copy(bf16[128,2048]{1,0:T(8,128)(2,1)S(1)} %shard_map.199) | data formatting | bytes 1048576
